TPU v7x, 32 devices: a whole 2x2x4 slice. The times are simulated.
32 devices in a mesh: sp: 4 (over z), fs: 4 (over y, x), tp: 2 (over core).
Axes of the slice: x: 2, y: 2, z: 4, core: 2. Of those that a mesh axis runs over, the one named last changes fastest.
Arguments:
- tokens: bfloat16 [4096, 2048], P('sp'), may hold values from -6 to 6
- norm_gain: float32 [2048], replicated, may hold values from 0.1 to 1.9
- w_query: bfloat16 [2048, 2048], P('sp', ('fs', 'tp')), may hold values from -3.6239223 to 3.6239223
- w_key: bfloat16 [2048, 512], P('sp', ('fs', 'tp')), may hold values from -0.088388348 to 0.088388348
- w_value: bfloat16 [2048, 512], P('sp', ('fs', 'tp')), may hold values from -0.8984375 to 0.8984375
- w_conv_in: bfloat16 [2048, 2048], P('sp', ('fs', 'tp')), may hold values from -0.125 to 0.125
- w_conv_gate: bfloat16 [2048, 2048], P('sp', ('fs', 'tp')), may hold values from -0.125 to 0.125
- conv_taps: bfloat16 [3, 2048], P(None, ('fs', 'tp')), may hold values from -3.5 to 3.5
- sink_logits: float32 [32], P(('fs', 'tp')), may hold values from 2 to 6
Outputs:
- mixed: bfloat16 [4096, 2048], P('sp', ('fs', 'tp'))
- log_sums: float32 [32, 4096], P(('fs', 'tp'), 'sp')
All inputs are finite; a program needn't handle non-finite values.
Results may differ from a plain program's by a relative error of at most 0.0077.
Values may be sent and summed in bfloat16 or wider, within the bound.
A program may use at most 64 MiB of HBM per device.

v0:
```python
import functools

import jax
import jax.numpy as jnp
from jax import lax
from jax.experimental import pallas as pl
from jax.experimental.pallas import tpu as pltpu
from jax.sharding import PartitionSpec as P

HEAD_DIM = 64
WINDOW = 128
TAPS = 3
EPS = 1e-06
LANES = 128
PAD = 8
MESH = pl.DeviceIdType.MESH


def kernel(
    n, flip, tok_ref, gain_ref, *refs
):
    arrays = 5 if flip else 4
    shards = refs[:arrays]
    (
        taps_ref, sink_ref, mixed_ref, log_ref,
        tok, normed, kv_all, q_all, ci_all, cg_all, kv, query, attended, conv_in, gate_sum,
        tok_sem, own_sem, recv_sem, right_sem, left_sem, halo_send, halo_recv,
    ) = refs[arrays:]
    QUERY, CONV, GATE = arrays - 3, arrays - 2, arrays - 1
    me = lax.axis_index("sp")
    rows = tok.shape[0]
    depth = shards[QUERY].shape[0]
    wholes = (kv_all, kv_all, q_all, ci_all, cg_all)[5 - arrays :]
    has_left, has_right = me > 0, me < n - 1
    left, right = jnp.maximum(me - 1, 0), jnp.minimum(me + 1, n - 1)
    blocks = rows // WINDOW
    f32, bf16 = jnp.float32, jnp.bfloat16

    step_rows = rows // 4
    tok_copies = [
        pltpu.make_async_copy(
            tok_ref.at[pl.ds(i * step_rows, step_rows)], tok.at[pl.ds(i * step_rows, step_rows)], tok_sem.at[i]
        )
        for i in range(4)
    ]
    for copy in tok_copies:
        copy.start()

    def place(a, shard):
        at = pl.ds(pl.multiple_of(shard * depth, depth), depth)
        if flip and a < QUERY:
            return kv_all.at[pl.ds(a * HEAD_DIM, HEAD_DIM), at]
        return wholes[a].at[at]

    own_copies = [pltpu.make_async_copy(shards[a], place(a, me), own_sem.at[a]) for a in range(arrays)]
    for copy in own_copies:
        copy.start()

    barrier = pltpu.get_barrier_semaphore()

    @pl.when(has_left)
    def _():
        pl.semaphore_signal(barrier, inc=1, device_id={"sp": left}, device_id_type=MESH)

    @pl.when(has_right)
    def _():
        pl.semaphore_signal(barrier, inc=1, device_id={"sp": right}, device_id_type=MESH)

    pl.semaphore_wait(barrier, has_left.astype(jnp.int32) + has_right.astype(jnp.int32))

    def hop(a, shard, to_right, own=False):
        return pltpu.make_async_remote_copy(
            src_ref=shards[a] if own else place(a, shard),
            dst_ref=place(a, shard),
            send_sem=(right_sem if to_right else left_sem).at[a, shard],
            recv_sem=recv_sem.at[a, shard],
            device_id={"sp": right if to_right else left},
            device_id_type=MESH,
        )

    def send_own(a):
        @pl.when(has_right)
        def _():
            hop(a, me, True, True).start()

        @pl.when(has_left)
        def _():
            hop(a, me, False, True).start()

    def pass_on(a, first, last):
        def step(k, carry):
            @pl.when(me - k >= 0)
            def _():
                shard = me - k
                hop(a, shard, False).wait_recv()

                @pl.when(has_right)
                def _():
                    hop(a, shard, True).start()

            @pl.when(me + k < n)
            def _():
                shard = me + k
                hop(a, shard, True).wait_recv()

                @pl.when(has_left)
                def _():
                    hop(a, shard, False).start()

            return carry

        lax.fori_loop(first, last, step, 0)

    for a in range(GATE):
        send_own(a)

    norm_rows = 64
    for i in range(4):
        tok_copies[i].wait()

        @pl.loop(0, step_rows // norm_rows)
        def _(j):
            at = pl.ds(pl.multiple_of(i * step_rows + j * norm_rows, norm_rows), norm_rows)
            wide = tok[at, :].astype(f32)
            scale = lax.rsqrt(jnp.mean(wide * wide, axis=-1, keepdims=True) + EPS)
            normed[at, :] = (wide * scale * gain_ref[...]).astype(bf16)

    for copy in own_copies:
        copy.wait()

    tile = 256

    def project(a, store):
        @pl.loop(0, rows // tile)
        def _(i):
            base = pl.multiple_of(i * tile, tile)
            side = 1 if flip and a < QUERY else 0
            store(
                base,
                lax.dot_general(
                    normed[pl.ds(base, tile), :],
                    wholes[a][...],
                    (((1,), (side,)), ((), ())),
                    preferred_element_type=f32,
                ),
            )

    def halo(buffer, length, i):
        return pltpu.make_async_remote_copy(
            src_ref=buffer.at[pl.ds(rows, length)],
            dst_ref=buffer.at[pl.ds(0, length)],
            send_sem=halo_send.at[i],
            recv_sem=halo_recv.at[i],
            device_id={"sp": right},
            device_id_type=MESH,
        )

    for a in range(QUERY):
        pass_on(a, 1, n)
    send_own(GATE)

    def store_kv(base, value):
        kv[pl.ds(base + WINDOW, tile), :] = value.astype(bf16)

    project(0, store_kv)

    @pl.when(jnp.logical_not(has_left))
    def _():
        kv[pl.ds(0, WINDOW), :] = jnp.zeros((WINDOW, kv.shape[1]), bf16)
        conv_in[pl.ds(0, PAD), :] = jnp.zeros((PAD, conv_in.shape[1]), f32)

    pass_on(QUERY, 1, n)

    @pl.when(has_right)
    def _():
        halo(kv, WINDOW, 0).start()

    def store_query(base, value):
        query[pl.ds(base, tile), :] = value.astype(bf16)

    project(QUERY, store_query)

    heads = query.shape[1] // HEAD_DIM
    query_idx = lax.broadcasted_iota(jnp.int32, (WINDOW, 2 * WINDOW), 0)
    key_idx = lax.broadcasted_iota(jnp.int32, (WINDOW, 2 * WINDOW), 1)
    gap = query_idx + WINDOW - key_idx
    band = (gap >= 0) & (gap < WINDOW)
    lane = lax.broadcasted_iota(jnp.int32, (2 * WINDOW, LANES), 1)
    low = lane < HEAD_DIM
    stat_lane = lax.broadcasted_iota(jnp.int32, (WINDOW, LANES), 1)

    def attend(b, kept):
        base = pl.multiple_of(b * WINDOW, WINDOW)
        both = kv[pl.ds(base, 2 * WINDOW), :].astype(f32)
        turned = pltpu.roll(both, HEAD_DIM, 1)
        zero = jnp.zeros_like(both)
        keys = (jnp.where(low, both, zero).astype(bf16), jnp.where(low, zero, turned).astype(bf16))
        vals = (jnp.where(low, turned, zero).astype(bf16), jnp.where(low, zero, both).astype(bf16))
        stats = jnp.zeros((WINDOW, LANES), f32)
        for pair in range(heads // 2):
            cols = pl.ds(pair * LANES, LANES)
            q = query[pl.ds(base, WINDOW), cols]
            out = None
            for side in range(2):
                head = 2 * pair + side
                scores = lax.dot_general(
                    q, keys[side], (((1,), (1,)), ((), ())), preferred_element_type=f32
                ) * HEAD_DIM ** (-0.5)
                scores = jnp.where(kept, scores, -jnp.inf)
                sink = jnp.full((WINDOW, 1), sink_ref[head], f32)
                top = jnp.maximum(jnp.max(scores, axis=-1, keepdims=True), sink)
                raised = jnp.exp(scores - top)
                total = jnp.sum(raised, axis=-1, keepdims=True) + jnp.exp(sink - top)
                weights = (raised * (1.0 / total)).astype(bf16)
                part = jnp.dot(weights, vals[side], preferred_element_type=f32)
                out = part if out is None else out + part
                stats = jnp.where(stat_lane == head, top + jnp.log(total), stats)
            attended[pl.ds(base, WINDOW), cols] = out
        log_ref[:, pl.ds(base, WINDOW)] = jnp.transpose(stats)[:heads]

    def attend_range(first, last):
        @pl.loop(first, last)
        def _(b):
            attend(b, band)

    cut = [1 + (n - 1) * i // 3 for i in range(4)]
    mid = 1 + (blocks - 1) // 2
    attend_range(1, mid)
    pass_on(CONV, cut[0], cut[1])
    attend_range(mid, blocks)
    pass_on(CONV, cut[1], cut[2])

    @pl.when(has_left)
    def _():
        halo(kv, WINDOW, 0).wait_recv()

    attend(0, band & ((key_idx >= WINDOW) | has_left))
    pass_on(CONV, cut[2], cut[3])

    def store_conv(base, value):
        conv_in[pl.ds(base + PAD, tile), :] = value.astype(bf16).astype(f32)

    project(CONV, store_conv)
    early = min(2, n - 1)
    pass_on(GATE, 1, early)

    @pl.when(has_right)
    def _():
        halo(conv_in, PAD, 1).start()

    pass_on(GATE, early, n - 1)

    far = jnp.where(2 * me >= n, 0, n - 1)

    def gate_part(base, shard):
        at = pl.ds(pl.multiple_of(shard * depth, depth), depth)
        return jnp.dot(
            normed[pl.ds(base, tile), at], cg_all[at, :], preferred_element_type=f32
        )

    if flip:

        @pl.loop(0, rows // tile)
        def _(i):
            base = pl.multiple_of(i * tile, tile)
            part = gate_part(base, lax.rem(far + 1, n))
            for j in range(2, n):
                part = part + gate_part(base, lax.rem(far + j, n))
            gate_sum[pl.ds(base, tile), :] = part

    pass_on(GATE, n - 1, n)

    @pl.when(has_left)
    def _():
        halo(conv_in, PAD, 1).wait_recv()

    def store_mixed(base, value):
        gate = value.astype(bf16).astype(f32)
        taps = taps_ref[...].astype(f32)
        near = conv_in[pl.ds(base, tile + PAD), :]
        total = jnp.zeros_like(gate)
        for k in range(TAPS):
            start = PAD - TAPS + 1 + k
            total = total + taps[k : k + 1] * near[start : start + tile]
        mixed_ref[pl.ds(base, tile), :] = (attended[pl.ds(base, tile), :] + gate * total).astype(bf16)

    if flip:

        @pl.loop(0, rows // tile)
        def _(i):
            base = pl.multiple_of(i * tile, tile)
            store_mixed(base, gate_sum[pl.ds(base, tile), :] + gate_part(base, far))

    else:
        project(GATE, store_mixed)

    @pl.when(has_right)
    def _():
        halo(kv, WINDOW, 0).wait_send()
        halo(conv_in, PAD, 1).wait_send()

    for a in range(arrays):

        @pl.when(has_right)
        def _():
            @pl.loop(0, me + 1)
            def _(s):
                hop(a, s, True).wait_send()

        @pl.when(has_left)
        def _():
            @pl.loop(me, n)
            def _(s):
                hop(a, s, False).wait_send()


def body(n, tokens, norm_gain, w_query, w_key, w_value, w_conv_in, w_conv_gate, conv_taps, sink_logits):
    rows, features = tokens.shape
    width, kv_width = w_query.shape[1], w_key.shape[1] + w_value.shape[1]
    assert w_key.shape[1] == HEAD_DIM and width % LANES == 0
    depth = w_query.shape[0]
    flip = depth % LANES == 0 and 2 < n <= 16
    if flip:
        w_kv, kv_shape = (w_key.T, w_value.T), (kv_width, features)
    else:
        w_kv, kv_shape = (jnp.concatenate([w_key, w_value], axis=1),), (features, kv_width)
    arrays = 3 + len(w_kv)
    f32, bf16 = jnp.float32, jnp.bfloat16
    hbm = pl.BlockSpec(memory_space=pltpu.HBM)
    vmem = pl.BlockSpec(memory_space=pltpu.VMEM)
    smem = pl.BlockSpec(memory_space=pltpu.SMEM)
    dma = pltpu.SemaphoreType.DMA
    return pl.pallas_call(
        functools.partial(kernel, n, flip),
        out_shape=(
            pltpu.VMEM((rows, width), bf16),
            pltpu.VMEM((width // HEAD_DIM, rows), f32),
        ),
        in_specs=[hbm, vmem] + [hbm] * arrays + [vmem, smem],
        out_specs=(vmem, vmem),
        scratch_shapes=[
            pltpu.VMEM((rows, features), bf16),
            pltpu.VMEM((rows, features), bf16),
            pltpu.VMEM(kv_shape, bf16),
            pltpu.VMEM((features, width), bf16),
            pltpu.VMEM((features, width), bf16),
            pltpu.VMEM((features, width), bf16),
            pltpu.VMEM((rows + WINDOW, kv_width), bf16),
            pltpu.VMEM((rows, width), bf16),
            pltpu.VMEM((rows, width), f32),
            pltpu.VMEM((rows + PAD, width), f32),
            pltpu.VMEM((rows, width), f32),
            dma((4,)),
            dma((arrays,)),
            dma((arrays, n)),
            dma((arrays, n)),
            dma((arrays, n)),
            dma((2,)),
            dma((2,)),
        ],
        compiler_params=pltpu.CompilerParams(
            collective_id=0, has_side_effects=True, vmem_limit_bytes=59 << 20
        ),
        name="gather_attend_convolve",
    )(tokens, norm_gain.reshape(1, -1), *w_kv, w_query, w_conv_in, w_conv_gate, conv_taps, sink_logits)


def solution(mesh):
    return jax.shard_map(
        functools.partial(body, mesh.shape["sp"]),
        mesh=mesh,
        in_specs=(
            P("sp", None),
            P(),
            P("sp", ("fs", "tp")),
            P("sp", ("fs", "tp")),
            P("sp", ("fs", "tp")),
            P("sp", ("fs", "tp")),
            P("sp", ("fs", "tp")),
            P(None, ("fs", "tp")),
            P(("fs", "tp")),
        ),
        out_specs=(P("sp", ("fs", "tp")), P(("fs", "tp"), "sp")),
        check_vma=False,
    )
```

profile of v0, /device:TPU:0, one launch (start us, length us, event | category | flops | bytes accessed | tf_op | source)
XLA Modules:
  0.0 70.6 jit_solution(18116916913069561802)
XLA Ops:
  0.6 68.6 %gather_attend_convolve.1 = (bf16[1024,256]{1,0:T(8,128)(2,1)S(1)}, f32[4,1024]{1,0:T(4,128)S(1)}) custom-call(bf16[1024,2048]{1,0:T(8,128)(2,1)} %tok_ref.1, f32[1,2048]{1,0:T(1,128)} %bitcast.5, bf16[64,512]{1,0:T(8,128)(2,1)} %bitcast.3, bf16[64,512]{1,0:T(8,128)(2,1)} %bitcast.4, bf16[512,256]{1,0:T(8,128)(2,1)} %refs_2_.1, bf16[512,256]{1,0:T(8,128)(2,1)} %refs_3_.1, ...), custom_call_target="tpu_custom_call" | custom-call | tf_op jit(solution)/shard_map/gather_attend_convolve/pallas_call | solution.py:333
  69.2 0.8 %copy.13 = bf16[1024,256]{1,0:T(8,128)(2,1)} copy(bf16[1024,256]{1,0:T(8,128)(2,1)S(1)} %get-tuple-element.2) | data formatting | bytes 1048576
  70.0 0.6 copy.14
where the time goes:
time: 70.9 us; the launch traced here: 70.6 us
  Pallas kernels  68.6 us (97%)
  local copies, waits for them, and re-layouts  1.4 us (2%)
    pallas_call x1, Pallas kernels, body(): pl.pallas_call(functools.partial(kernel, n, flip), out_shape=(pltpu.VMEM(...  68.6 us

commit v1 on v0

--- a/solution.py
+++ b/solution.py
@@ -16,7 +16,7 @@
 MESH = pl.DeviceIdType.MESH
 
 
-def kernel(
+def line_kernel(
     n, flip, tok_ref, gain_ref, *refs
 ):
     arrays = 5 if flip else 4
@@ -314,7 +314,541 @@
                 hop(a, s, False).wait_send()
 
 
-def body(n, tokens, norm_gain, w_query, w_key, w_value, w_conv_in, w_conv_gate, conv_taps, sink_logits):
+def paired_kernel(tok_ref, gain_ref, *refs):
+    shards = refs[:5]
+    (
+        taps_ref, sink_ref, mixed_ref, log_ref,
+        tok, normed, other, kv_all, q_all, conv_w0, conv_w1, kv, query, q_part, attended,
+        conv_in0, conv_in1, gates, sums, conv_out, conv_back,
+        tok_sem, own_sem, recv_sem, mate_sem, peer_sem, halo_send, halo_recv,
+        x_send, x_recv, out_send, out_recv,
+    ) = refs[5:]
+    conv_w, conv_in = (conv_w0, conv_w1), (conv_in0, conv_in1)
+    f32, bf16 = jnp.float32, jnp.bfloat16
+    me, fs, tp = lax.axis_index("sp"), lax.axis_index("fs"), lax.axis_index("tp")
+    low = me < 2
+    end = (me == 0) | (me == 3)
+    middle = jnp.logical_not(end)
+    mate = me + 1 - 2 * lax.rem(me, 2)
+    peer = jnp.where(end, 3 - mate, 3 - me)
+    far = jnp.where(low, 3, 0)
+    first = jnp.where(low, 0, 1)
+    has_left, has_right = me > 0, me < 3
+    right = jnp.minimum(me + 1, 3)
+    across, along = fs + 1 - 2 * lax.rem(fs, 2), lax.rem(fs + 2, 4)
+    diagonal = 3 - fs
+    twin = 1 - tp
+    rows = tok.shape[0]
+    depth = shards[2].shape[0]
+    blocks = rows // WINDOW
+    K, V, Q, CI0, CG0, CI1, CG1 = range(7)
+
+    parts = 8
+    part_rows = rows // parts
+    piece = part_rows // 2
+    own_part = fs * 2 + tp
+
+    def part_at(i):
+        return lax.rem(own_part + i, parts)
+
+    def rows_of(start, length):
+        return pl.ds(pl.multiple_of(start, 16), length)
+
+    tok_copies = []
+    for i in range(parts):
+        at = rows_of(part_at(i) * part_rows, part_rows)
+        tok_copies.append(pltpu.make_async_copy(tok_ref.at[at], tok.at[at], tok_sem.at[i]))
+    for copy in tok_copies:
+        copy.start()
+
+    def source(u):
+        if u <= Q:
+            return shards[u]
+        half = (u - CI0) // 2
+        return shards[3 + (u - CI0) % 2].at[:, pl.ds(half * LANES, LANES)]
+
+    def place(u, shard):
+        at = pl.ds(pl.multiple_of(shard * depth, depth), depth)
+        if u < Q:
+            return kv_all.at[pl.ds(u * HEAD_DIM, HEAD_DIM), at]
+        if u == Q:
+            return q_all.at[at]
+        return conv_w[(u - CI0) // 2].at[at, pl.ds((u - CI0) % 2 * LANES, LANES)]
+
+    own_copies = [pltpu.make_async_copy(source(u), place(u, me), own_sem.at[u]) for u in range(7)]
+    for u in (K, V, Q):
+        own_copies[u].start()
+
+    @pl.when(middle)
+    def _():
+        for u in (CI0, CG0, CI1, CG1):
+            own_copies[u].start()
+
+    barrier = pltpu.get_barrier_semaphore()
+
+    def greet(**device):
+        pl.semaphore_signal(barrier, inc=1, device_id=device, device_id_type=MESH)
+
+    greet(sp=mate)
+
+    @pl.when(middle)
+    def _():
+        greet(sp=peer)
+        greet(fs=across)
+        greet(fs=along)
+        greet(tp=twin)
+
+    pl.semaphore_wait(barrier, jnp.where(middle, 5, 1))
+
+    def hop(u, shard, to_mate, own=False):
+        return pltpu.make_async_remote_copy(
+            src_ref=source(u) if own else place(u, shard),
+            dst_ref=place(u, shard),
+            send_sem=(mate_sem if to_mate else peer_sem).at[u, shard],
+            recv_sem=recv_sem.at[u, shard],
+            device_id={"sp": mate if to_mate else peer},
+            device_id_type=MESH,
+        )
+
+    def arrived(u, shard):
+        hop(u, shard, True).wait_recv()
+
+    for u in (K, V, Q):
+        hop(u, me, True, True).start()
+
+    @pl.when(middle)
+    def _():
+        for u in (K, V, Q):
+            hop(u, me, False, True).start()
+
+    def norm_part(i):
+        tok_copies[i].wait()
+        norm_rows = 64
+
+        @pl.loop(0, part_rows // norm_rows)
+        def _(j):
+            at = rows_of(part_at(i) * part_rows + j * norm_rows, norm_rows)
+            wide = tok[at, :].astype(f32)
+            scale = lax.rsqrt(jnp.mean(wide * wide, axis=-1, keepdims=True) + EPS)
+            normed[at, :] = (wide * scale * gain_ref[...]).astype(bf16)
+
+    def piece_at(part, h):
+        return rows_of(part * part_rows + h * piece, piece)
+
+    def piece_copy(buffer, part, h, i, **device):
+        at = piece_at(part, h)
+        return pltpu.make_async_remote_copy(
+            src_ref=buffer.at[at],
+            dst_ref=other.at[at],
+            send_sem=x_send.at[i],
+            recv_sem=x_recv.at[part * 2 + h],
+            device_id=device,
+            device_id_type=MESH,
+        )
+
+    def piece_arrived(part, h):
+        piece_copy(other, part, h, 0, sp=mate).wait_recv()
+
+    across_part, along_part, diagonal_part = across * 2 + tp, along * 2 + tp, diagonal * 2 + tp
+    relays = (
+        (own_part, 0, ("tp", "fs_across", "fs_along")),
+        (own_part, 1, ("tp", "fs_across", "fs_along")),
+        (across_part, 0, ("tp", "fs_along")),
+        (along_part, 0, ("tp",)),
+        (across_part, 1, ("tp",)),
+        (along_part, 1, ("tp", "fs_across")),
+        (diagonal_part, 0, ("tp",)),
+        (diagonal_part, 1, ("tp",)),
+    )
+    devices = {"tp": {"tp": twin}, "fs_across": {"fs": across}, "fs_along": {"fs": along}}
+
+    def relay_copies(j):
+        base = sum(len(to) for _, _, to in relays[:j])
+        part, h, to = relays[j]
+        return [piece_copy(other, part, h, base + i, **devices[d]) for i, d in enumerate(to)]
+
+    def relay(j):
+        piece_arrived(relays[j][0], relays[j][1])
+        for copy in relay_copies(j):
+            copy.start()
+
+    norm_part(0)
+    norm_part(1)
+
+    @pl.when(end)
+    def _():
+        for h in range(2):
+            piece_copy(normed, own_part, h, h, sp=mate).start()
+        for u in (CI0, CG0, CI1, CG1):
+            hop(u, me, True, True).start()
+
+    for i in range(2, parts):
+        norm_part(i)
+
+    for u in (K, V, Q):
+        own_copies[u].wait()
+
+    for u in (K, V):
+        arrived(u, mate)
+
+        @pl.when(middle)
+        def _():
+            hop(u, mate, False).start()
+
+        arrived(u, peer)
+
+        @pl.when(middle)
+        def _():
+            hop(u, peer, True).start()
+
+    arrived(Q, mate)
+
+    @pl.when(middle)
+    def _():
+        hop(Q, mate, False).start()
+        for u in (CI0, CG0, CI1):
+            hop(u, me, False, True).start()
+
+    arrived(Q, peer)
+
+    @pl.when(middle)
+    def _():
+        hop(Q, peer, True).start()
+
+    for u in (K, V):
+        arrived(u, far)
+
+        @pl.when(middle)
+        def _():
+            hop(u, far, True).start()
+
+    tile = 256
+
+    @pl.loop(0, rows // tile)
+    def _(i):
+        base = pl.multiple_of(i * tile, tile)
+        kv[pl.ds(base + WINDOW, tile), :] = lax.dot_general(
+            normed[pl.ds(base, tile), :], kv_all[...], (((1,), (1,)), ((), ())), preferred_element_type=f32
+        ).astype(bf16)
+
+    def halo(buffer, start, length, i):
+        return pltpu.make_async_remote_copy(
+            src_ref=buffer.at[pl.ds(start, length)],
+            dst_ref=buffer.at[pl.ds(0, length)],
+            send_sem=halo_send.at[i],
+            recv_sem=halo_recv.at[i],
+            device_id={"sp": right},
+            device_id_type=MESH,
+        )
+
+    kv_halo = halo(kv, rows, WINDOW, 0)
+
+    @pl.when(jnp.logical_not(has_left))
+    def _():
+        kv[pl.ds(0, WINDOW), :] = jnp.zeros((WINDOW, kv.shape[1]), bf16)
+
+    early = pl.ds(pl.multiple_of(first * depth, depth), 3 * depth)
+    late = pl.ds(pl.multiple_of(far * depth, depth), depth)
+
+    @pl.loop(0, rows // tile)
+    def _(i):
+        at = pl.ds(pl.multiple_of(i * tile, tile), tile)
+        q_part[at, :] = jnp.dot(normed[at, early], q_all[early, :], preferred_element_type=f32)
+
+    @pl.when(has_right)
+    def _():
+        kv_halo.start()
+
+    @pl.when(middle)
+    def _():
+        relay(0)
+
+    arrived(Q, far)
+
+    @pl.when(middle)
+    def _():
+        hop(Q, far, True).start()
+
+    @pl.loop(0, rows // tile)
+    def _(i):
+        at = pl.ds(pl.multiple_of(i * tile, tile), tile)
+        query[at, :] = (
+            q_part[at, :] + jnp.dot(normed[at, late], q_all[late, :], preferred_element_type=f32)
+        ).astype(bf16)
+
+    heads = query.shape[1] // HEAD_DIM
+    query_idx = lax.broadcasted_iota(jnp.int32, (WINDOW, 2 * WINDOW), 0)
+    key_idx = lax.broadcasted_iota(jnp.int32, (WINDOW, 2 * WINDOW), 1)
+    gap = query_idx + WINDOW - key_idx
+    band = (gap >= 0) & (gap < WINDOW)
+    lane = lax.broadcasted_iota(jnp.int32, (2 * WINDOW, LANES), 1)
+    low_lanes = lane < HEAD_DIM
+    stat_lane = lax.broadcasted_iota(jnp.int32, (WINDOW, LANES), 1)
+
+    def attend(b, kept):
+        base = pl.multiple_of(b * WINDOW, WINDOW)
+        both = kv[pl.ds(base, 2 * WINDOW), :].astype(f32)
+        turned = pltpu.roll(both, HEAD_DIM, 1)
+        zero = jnp.zeros_like(both)
+        keys = (jnp.where(low_lanes, both, zero).astype(bf16), jnp.where(low_lanes, zero, turned).astype(bf16))
+        vals = (jnp.where(low_lanes, turned, zero).astype(bf16), jnp.where(low_lanes, zero, both).astype(bf16))
+        stats = jnp.zeros((WINDOW, LANES), f32)
+        for pair in range(heads // 2):
+            cols = pl.ds(pair * LANES, LANES)
+            q = query[pl.ds(base, WINDOW), cols]
+            out = None
+            for side in range(2):
+                head = 2 * pair + side
+                scores = lax.dot_general(
+                    q, keys[side], (((1,), (1,)), ((), ())), preferred_element_type=f32
+                ) * HEAD_DIM ** (-0.5)
+                scores = jnp.where(kept, scores, -jnp.inf)
+                sink = jnp.full((WINDOW, 1), sink_ref[head], f32)
+                top = jnp.maximum(jnp.max(scores, axis=-1, keepdims=True), sink)
+                raised = jnp.exp(scores - top)
+                total = jnp.sum(raised, axis=-1, keepdims=True) + jnp.exp(sink - top)
+                weights = (raised * (1.0 / total)).astype(bf16)
+                part = jnp.dot(weights, vals[side], preferred_element_type=f32)
+                out = part if out is None else out + part
+                stats = jnp.where(stat_lane == head, top + jnp.log(total), stats)
+            attended[pl.ds(base, WINDOW), cols] = out
+        log_ref[:, pl.ds(base, WINDOW)] = jnp.transpose(stats)[:heads]
+
+    def forward_conv(u):
+        arrived(u, mate)
+        hop(u, mate, False).start()
+
+    def relay_far():
+        forward_conv(CG0)
+        hop(CG1, me, False, True).start()
+
+    services = (
+        (lambda: relay(1),),
+        (lambda: relay(2), lambda: relay(3)),
+        (lambda: forward_conv(CI0),),
+        (relay_far,),
+        (lambda: relay(4), lambda: relay(5)),
+    )
+    cuts = [1 + (blocks - 1) * i // len(services) for i in range(len(services) + 1)]
+    for i, jobs in enumerate(services):
+
+        @pl.loop(cuts[i], cuts[i + 1])
+        def _(b):
+            attend(b, band)
+
+        @pl.when(middle)
+        def _():
+            for job in jobs:
+                job()
+
+    @pl.when(has_left)
+    def _():
+        kv_halo.wait_recv()
+
+    attend(0, band & ((key_idx >= WINDOW) | has_left))
+
+    own_base, mate_base = jnp.where(me == 1, rows, 0), jnp.where(me == 1, 0, rows)
+    tiles = rows // tile
+
+    def seq(base, i):
+        return pl.multiple_of(base + i * tile, tile)
+
+    def out_copy(half, i):
+        at = (pl.ds(i * tile, tile), pl.ds(half * LANES, LANES))
+        return pltpu.make_async_remote_copy(
+            src_ref=conv_out.at[at],
+            dst_ref=conv_back.at[at],
+            send_sem=out_send.at[half * tiles + i],
+            recv_sem=out_recv.at[half * tiles + i],
+            device_id={"sp": mate},
+            device_id_type=MESH,
+        )
+
+    def convolve(half, at, gate):
+        taps = taps_ref[:, pl.ds(half * LANES, LANES)].astype(f32)
+        near = conv_in[half][pl.ds(at, tile + PAD), :]
+        total = jnp.zeros((tile, LANES), f32)
+        for k in range(TAPS):
+            start = PAD - TAPS + 1 + k
+            total = total + taps[k : k + 1] * near[start : start + tile]
+        return gate * total
+
+    def split(half, at, value):
+        value = value.astype(bf16).astype(f32)
+        conv_in[half][pl.ds(at + PAD, tile), :] = value[:, :LANES]
+        return value[:, LANES:]
+
+    def convolution(half, product):
+        def own_product(i):
+            gates[pl.ds(i * tile, tile), :] = split(half, seq(own_base, i), product(0, i))
+
+        own_product(tiles - 1)
+
+        @pl.when(me == 1)
+        def _():
+            conv_in[half][pl.ds(0, PAD), :] = jnp.zeros((PAD, LANES), f32)
+            halo(conv_in[half], 2 * rows, PAD, 1 + half).start()
+
+        cols = pl.ds(half * LANES, LANES)
+        for i in range(tiles):
+            at = seq(mate_base, i)
+            gate = split(half, at, product(1, i))
+            conv_out[pl.ds(i * tile, tile), cols] = convolve(half, at, gate).astype(bf16)
+            out_copy(half, i).start()
+        for i in range(tiles - 1):
+            own_product(i)
+
+        @pl.when(me == 2)
+        def _():
+            halo(conv_in[half], 2 * rows, PAD, 1 + half).wait_recv()
+
+        for i in range(tiles):
+            at = pl.ds(i * tile, tile)
+            convolved = convolve(half, seq(own_base, i), gates[at, :])
+            mixed_ref[at, cols] = (attended[at, cols] + convolved).astype(bf16)
+
+    sources = (normed, other)
+
+    @pl.when(middle)
+    def _():
+        for u in (CI0, CG0, CI1, CG1):
+            own_copies[u].wait()
+        forward_conv(CI1)
+        for shard in (peer, far):
+            for u in (CI0, CG0):
+                arrived(u, shard)
+        forward_conv(CG1)
+        relay(6)
+        relay(7)
+        for part in (fs * 2 + twin, across * 2 + twin, along * 2 + twin, diagonal * 2 + twin):
+            for h in range(2):
+                piece_arrived(part, h)
+
+        def whole(which, i):
+            at = pl.ds(i * tile, tile)
+            return jnp.dot(sources[which][at, :], conv_w0[...], preferred_element_type=f32)
+
+        convolution(0, whole)
+        for u in (CI1, CG1):
+            arrived(u, peer)
+        for which in range(2):
+
+            @pl.loop(0, tiles)
+            def _(i):
+                at = pl.ds(pl.multiple_of(i * tile, tile), tile)
+                sums[which, at, :] = jnp.dot(
+                    sources[which][at, early], conv_w1[early, :], preferred_element_type=f32
+                )
+
+        for u in (CI1, CG1):
+            arrived(u, far)
+
+        def finish(which, i):
+            at = pl.ds(i * tile, tile)
+            return sums[which, at, :] + jnp.dot(
+                sources[which][at, late], conv_w1[late, :], preferred_element_type=f32
+            )
+
+        convolution(1, finish)
+
+    @pl.when(end)
+    def _():
+        for half in range(2):
+            for i in range(tiles):
+                at = (pl.ds(i * tile, tile), pl.ds(half * LANES, LANES))
+                out_copy(half, i).wait_recv()
+                mixed_ref[at] = (attended[at] + conv_back[at].astype(f32)).astype(bf16)
+
+    @pl.when(has_right)
+    def _():
+        kv_halo.wait_send()
+
+    for u in (K, V, Q):
+        hop(u, me, True, True).wait_send()
+
+    @pl.when(end)
+    def _():
+        for h in range(2):
+            piece_copy(normed, own_part, h, h, sp=mate).wait_send()
+        for u in (CI0, CG0, CI1, CG1):
+            hop(u, me, True, True).wait_send()
+
+    @pl.when(middle)
+    def _():
+        for u in (K, V, Q):
+            hop(u, peer, True).wait_send()
+            hop(u, far, True).wait_send()
+        for u in range(7):
+            hop(u, me, False, True).wait_send()
+            hop(u, mate, False).wait_send()
+        for j in range(len(relays)):
+            for copy in relay_copies(j):
+                copy.wait_send()
+        for half in range(2):
+            for i in range(tiles):
+                out_copy(half, i).wait_send()
+
+        @pl.when(me == 1)
+        def _():
+            for half in range(2):
+                halo(conv_in[half], 2 * rows, PAD, 1 + half).wait_send()
+
+
+def paired_body(tokens, norm_gain, w_query, w_key, w_value, w_conv_in, w_conv_gate, conv_taps, sink_logits):
+    rows, features = tokens.shape
+    width = w_query.shape[1]
+    f32, bf16 = jnp.float32, jnp.bfloat16
+    hbm = pl.BlockSpec(memory_space=pltpu.HBM)
+    vmem = pl.BlockSpec(memory_space=pltpu.VMEM)
+    smem = pl.BlockSpec(memory_space=pltpu.SMEM)
+    dma = pltpu.SemaphoreType.DMA
+    tiles = rows // 256
+    return pl.pallas_call(
+        paired_kernel,
+        out_shape=(
+            pltpu.VMEM((rows, width), bf16),
+            pltpu.VMEM((width // HEAD_DIM, rows), f32),
+        ),
+        in_specs=[hbm, vmem] + [hbm] * 5 + [vmem, smem],
+        out_specs=(vmem, vmem),
+        scratch_shapes=[
+            pltpu.VMEM((rows, features), bf16),
+            pltpu.VMEM((rows, features), bf16),
+            pltpu.VMEM((rows, features), bf16),
+            pltpu.VMEM((2 * HEAD_DIM, features), bf16),
+            pltpu.VMEM((features, width), bf16),
+            pltpu.VMEM((features, width), bf16),
+            pltpu.VMEM((features, width), bf16),
+            pltpu.VMEM((rows + WINDOW, 2 * HEAD_DIM), bf16),
+            pltpu.VMEM((rows, width), bf16),
+            pltpu.VMEM((rows, width), f32),
+            pltpu.VMEM((rows, width), f32),
+            pltpu.VMEM((2 * rows + PAD, LANES), f32),
+            pltpu.VMEM((2 * rows + PAD, LANES), f32),
+            pltpu.VMEM((rows, LANES), f32),
+            pltpu.VMEM((2, rows, width), f32),
+            pltpu.VMEM((rows, width), bf16),
+            pltpu.VMEM((rows, width), bf16),
+            dma((8,)),
+            dma((7,)),
+            dma((7, 4)),
+            dma((7, 4)),
+            dma((7, 4)),
+            dma((3,)),
+            dma((3,)),
+            dma((14,)),
+            dma((16,)),
+            dma((2 * tiles,)),
+            dma((2 * tiles,)),
+        ],
+        compiler_params=pltpu.CompilerParams(
+            collective_id=0, has_side_effects=True, vmem_limit_bytes=59 << 20
+        ),
+        name="paired_attend_convolve",
+    )(tokens, norm_gain.reshape(1, -1), w_key.T, w_value.T, w_query, w_conv_in, w_conv_gate, conv_taps, sink_logits)
+
+
+def line_body(n, tokens, norm_gain, w_query, w_key, w_value, w_conv_in, w_conv_gate, conv_taps, sink_logits):
     rows, features = tokens.shape
     width, kv_width = w_query.shape[1], w_key.shape[1] + w_value.shape[1]
     assert w_key.shape[1] == HEAD_DIM and width % LANES == 0
@@ -331,7 +865,7 @@
     smem = pl.BlockSpec(memory_space=pltpu.SMEM)
     dma = pltpu.SemaphoreType.DMA
     return pl.pallas_call(
-        functools.partial(kernel, n, flip),
+        functools.partial(line_kernel, n, flip),
         out_shape=(
             pltpu.VMEM((rows, width), bf16),
             pltpu.VMEM((width // HEAD_DIM, rows), f32),
@@ -365,9 +899,17 @@
     )(tokens, norm_gain.reshape(1, -1), *w_kv, w_query, w_conv_in, w_conv_gate, conv_taps, sink_logits)
 
 
+def body(n, fs, tp, *arrays):
+    rows, width, depth = arrays[0].shape[0], arrays[2].shape[1], arrays[2].shape[0]
+    square = n == 4 and fs == 4 and tp == 2
+    if square and width == 2 * LANES and depth % LANES == 0 and rows % (8 * LANES) == 0:
+        return paired_body(*arrays)
+    return line_body(n, *arrays)
+
+
 def solution(mesh):
     return jax.shard_map(
-        functools.partial(body, mesh.shape["sp"]),
+        functools.partial(body, mesh.shape["sp"], mesh.shape["fs"], mesh.shape["tp"]),
         mesh=mesh,
         in_specs=(
             P("sp", None),

time: 70.9 us -> 60.8 us (0.86)
  Pallas kernels: 68.6 us -> 58.4 us
    pallas_call x1, Pallas kernels: 68.6 us -> 58.4 us  [paired_body(): pl.pallas_call(paired_kernel, out_shape=(pltpu.VMEM((rows, width), bf16),...]
where the time goes in v1:
time: 60.8 us; the launch traced here: 60.5 us
  Pallas kernels  58.4 us (96%)
  local copies, waits for them, and re-layouts  1.4 us (2%)
  between operations  0.64 us (1%)
    pallas_call x1, Pallas kernels, paired_body(): pl.pallas_call(paired_kernel, out_shape=(pltpu.VMEM((rows, width), bf16),...  58.4 us
    unnamed x2, local copies, waits for them, and re-layouts  1.4 us

profile of v1, /device:TPU:0, one launch (start us, length us, event | category | flops | bytes accessed | tf_op | source)
XLA Modules:
  0.0 60.5 jit_solution(2234443818025039488)
XLA Ops:
  0.6 58.4 %paired_attend_convolve.1 = (bf16[1024,256]{1,0:T(8,128)(2,1)S(1)}, f32[4,1024]{1,0:T(4,128)S(1)}) custom-call(bf16[1024,2048]{1,0:T(8,128)(2,1)} %tok_ref.1, f32[1,2048]{1,0:T(1,128)} %bitcast.5, bf16[64,512]{1,0:T(8,128)(2,1)} %bitcast.3, bf16[64,512]{1,0:T(8,128)(2,1)} %bitcast.4, bf16[512,256]{1,0:T(8,128)(2,1)} %refs_2_.1, bf16[512,256]{1,0:T(8,128)(2,1)} %refs_3_.1, ...), custom_call_target="tpu_custom_call" | custom-call | tf_op jit(solution)/shard_map/paired_attend_convolve/pallas_call | solution.py:806
  59.1 0.8 %copy.13 = bf16[1024,256]{1,0:T(8,128)(2,1)} copy(bf16[1024,256]{1,0:T(8,128)(2,1)S(1)} %get-tuple-element.2) | data formatting | bytes 1048576
  59.9 0.6 %copy.14 = f32[4,1024]{1,0:T(4,128)} copy(f32[4,1024]{1,0:T(4,128)S(1)} %get-tuple-element.3) | data formatting | bytes 32768

commit v2 on v1

--- a/solution.py
+++ b/solution.py
@@ -318,12 +318,11 @@
     shards = refs[:5]
     (
         taps_ref, sink_ref, mixed_ref, log_ref,
-        tok, normed, other, kv_all, q_all, conv_w0, conv_w1, kv, query, q_part, attended,
-        conv_in0, conv_in1, gates, sums, conv_out, conv_back,
+        tok, normed, other, kv_all, q_all, stage, conv_w, kv, query, q_part, attended,
+        conv_in, gates, convolved, sums, conv_out, conv_back, turned_taps, edge_out, edge_in,
         tok_sem, own_sem, recv_sem, mate_sem, peer_sem, halo_send, halo_recv,
         x_send, x_recv, out_send, out_recv,
     ) = refs[5:]
-    conv_w, conv_in = (conv_w0, conv_w1), (conv_in0, conv_in1)
     f32, bf16 = jnp.float32, jnp.bfloat16
     me, fs, tp = lax.axis_index("sp"), lax.axis_index("fs"), lax.axis_index("tp")
     low = me < 2
@@ -341,7 +340,14 @@
     rows = tok.shape[0]
     depth = shards[2].shape[0]
     blocks = rows // WINDOW
-    K, V, Q, CI0, CG0, CI1, CG1 = range(7)
+    width = q_all.shape[1]
+    widths = (width // 2, width // 4, width // 8, width // 8)
+    groups = range(len(widths))
+    channel = [sum(widths[:g]) for g in groups]
+    K, V, Q, G0, G0_GATE, G1, G2, G3 = units = range(8)
+    spans = {G0: (0, width // 2), G0_GATE: (width // 2, width // 2)}
+    spans.update({G0_GATE + g: (2 * channel[g], 2 * widths[g]) for g in groups[1:]})
+    units_of = ((G0, G0_GATE), (G1,), (G2,), (G3,))
 
     parts = 8
     part_rows = rows // parts
@@ -361,28 +367,21 @@
     for copy in tok_copies:
         copy.start()
 
-    def source(u):
-        if u <= Q:
-            return shards[u]
-        half = (u - CI0) // 2
-        return shards[3 + (u - CI0) % 2].at[:, pl.ds(half * LANES, LANES)]
+    def shard_at(shard):
+        return pl.ds(pl.multiple_of(shard * depth, depth), depth)
 
     def place(u, shard):
-        at = pl.ds(pl.multiple_of(shard * depth, depth), depth)
+        at = shard_at(shard)
         if u < Q:
             return kv_all.at[pl.ds(u * HEAD_DIM, HEAD_DIM), at]
         if u == Q:
             return q_all.at[at]
-        return conv_w[(u - CI0) // 2].at[at, pl.ds((u - CI0) % 2 * LANES, LANES)]
-
-    own_copies = [pltpu.make_async_copy(source(u), place(u, me), own_sem.at[u]) for u in range(7)]
-    for u in (K, V, Q):
-        own_copies[u].start()
-
-    @pl.when(middle)
-    def _():
-        for u in (CI0, CG0, CI1, CG1):
-            own_copies[u].start()
+        return conv_w.at[pl.ds(*spans[u]), at]
+
+    own_copies = [pltpu.make_async_copy(shards[u], place(u, me), own_sem.at[u]) for u in (K, V, Q)]
+    own_copies += [pltpu.make_async_copy(shards[3 + j], stage.at[j], own_sem.at[3 + j]) for j in range(2)]
+    for copy in own_copies:
+        copy.start()
 
     barrier = pltpu.get_barrier_semaphore()
 
@@ -398,11 +397,25 @@
         greet(fs=along)
         greet(tp=twin)
 
+    own_copies[3].wait()
+    own_copies[4].wait()
+    for j in range(2):
+        for block in range(depth // LANES):
+            turned = jnp.transpose(stage[j, pl.ds(block * LANES, LANES), :].astype(f32)).astype(bf16)
+            at = pl.ds(pl.multiple_of(me * depth + block * LANES, LANES), LANES)
+            for g in groups:
+                to = pl.ds(2 * channel[g] + j * widths[g], widths[g])
+                conv_w[to, at] = turned[channel[g] : channel[g] + widths[g]]
+    taps = taps_ref[...].astype(f32)
+    turned_taps[...] = jnp.transpose(jnp.concatenate([taps, jnp.zeros((8 - TAPS, width), f32)], axis=0))
+    for u in (K, V, Q):
+        own_copies[u].wait()
+
     pl.semaphore_wait(barrier, jnp.where(middle, 5, 1))
 
-    def hop(u, shard, to_mate, own=False):
+    def hop(u, shard, to_mate):
         return pltpu.make_async_remote_copy(
-            src_ref=source(u) if own else place(u, shard),
+            src_ref=place(u, shard),
             dst_ref=place(u, shard),
             send_sem=(mate_sem if to_mate else peer_sem).at[u, shard],
             recv_sem=recv_sem.at[u, shard],
@@ -414,12 +427,12 @@
         hop(u, shard, True).wait_recv()
 
     for u in (K, V, Q):
-        hop(u, me, True, True).start()
+        hop(u, me, True).start()
 
     @pl.when(middle)
     def _():
         for u in (K, V, Q):
-            hop(u, me, False, True).start()
+            hop(u, me, False).start()
 
     def norm_part(i):
         tok_copies[i].wait()
@@ -479,14 +492,11 @@
     def _():
         for h in range(2):
             piece_copy(normed, own_part, h, h, sp=mate).start()
-        for u in (CI0, CG0, CI1, CG1):
-            hop(u, me, True, True).start()
+        for u in units[G0:]:
+            hop(u, me, True).start()
 
     for i in range(2, parts):
         norm_part(i)
-
-    for u in (K, V, Q):
-        own_copies[u].wait()
 
     for u in (K, V):
         arrived(u, mate)
@@ -506,8 +516,8 @@
     @pl.when(middle)
     def _():
         hop(Q, mate, False).start()
-        for u in (CI0, CG0, CI1):
-            hop(u, me, False, True).start()
+        for u in (G0, G0_GATE, G1):
+            hop(u, me, False).start()
 
     arrived(Q, peer)
 
@@ -618,15 +628,16 @@
         arrived(u, mate)
         hop(u, mate, False).start()
 
-    def relay_far():
-        forward_conv(CG0)
-        hop(CG1, me, False, True).start()
+    def forward_rest():
+        forward_conv(G1)
+        hop(G2, me, False).start()
+        hop(G3, me, False).start()
 
     services = (
         (lambda: relay(1),),
         (lambda: relay(2), lambda: relay(3)),
-        (lambda: forward_conv(CI0),),
-        (relay_far,),
+        (lambda: forward_conv(G0),),
+        (lambda: forward_conv(G0_GATE),),
         (lambda: relay(4), lambda: relay(5)),
     )
     cuts = [1 + (blocks - 1) * i // len(services) for i in range(len(services) + 1)]
@@ -648,150 +659,218 @@
     attend(0, band & ((key_idx >= WINDOW) | has_left))
 
     own_base, mate_base = jnp.where(me == 1, rows, 0), jnp.where(me == 1, 0, rows)
+    bases = (own_base, mate_base)
+    sources = (normed, other)
     tiles = rows // tile
-
-    def seq(base, i):
-        return pl.multiple_of(base + i * tile, tile)
-
-    def out_copy(half, i):
-        at = (pl.ds(i * tile, tile), pl.ds(half * LANES, LANES))
+    OWN, MATE = 0, 1
+    last = tiles - 1
+    pair = pl.ds(pl.multiple_of(jnp.minimum(me, mate) * depth, depth), 2 * depth)
+    rest = pl.ds(pl.multiple_of(jnp.minimum(peer, far) * depth, depth), 2 * depth)
+
+    def tile_at(i):
+        return pl.ds(i * tile if isinstance(i, int) else pl.multiple_of(i * tile, tile), tile)
+
+    def out_copy(g, i):
+        at = (pl.ds(channel[g], widths[g]), tile_at(i))
         return pltpu.make_async_remote_copy(
             src_ref=conv_out.at[at],
             dst_ref=conv_back.at[at],
-            send_sem=out_send.at[half * tiles + i],
-            recv_sem=out_recv.at[half * tiles + i],
+            send_sem=out_send.at[g * tiles + i],
+            recv_sem=out_recv.at[g * tiles + i],
             device_id={"sp": mate},
             device_id_type=MESH,
         )
 
-    def convolve(half, at, gate):
-        taps = taps_ref[:, pl.ds(half * LANES, LANES)].astype(f32)
-        near = conv_in[half][pl.ds(at, tile + PAD), :]
-        total = jnp.zeros((tile, LANES), f32)
+    def edge_copy(g):
+        return pltpu.make_async_remote_copy(
+            src_ref=edge_out.at[g],
+            dst_ref=edge_in.at[g],
+            send_sem=halo_send.at[1 + g],
+            recv_sem=halo_recv.at[1 + g],
+            device_id={"sp": right},
+            device_id_type=MESH,
+        )
+
+    def dot(which, i, start, length, at):
+        return lax.dot_general(
+            conv_w[pl.ds(start, length), at],
+            sources[which][tile_at(i), at],
+            (((1,), (1,)), ((), ())),
+            preferred_element_type=f32,
+        )
+
+    def partial(which, i, g, at, fresh):
+        start = 2 * channel[g]
+        value = dot(which, i, start, 2 * width - start, at)
+        to = pl.ds(start - 2 * widths[0], 2 * width - start)
+        sums[which, to, tile_at(i)] = value if fresh else sums[which, to, tile_at(i)] + value
+
+    def product(which, i, g, at):
+        value = dot(which, i, 2 * channel[g], 2 * widths[g], at)
+        if g:
+            value = value + sums[which, pl.ds(2 * channel[g] - 2 * widths[0], 2 * widths[g]), tile_at(i)]
+        value = value.astype(bf16).astype(f32)
+        base = pl.multiple_of(bases[which] + LANES + i * tile, LANES)
+        conv_in[pl.ds(channel[g], widths[g]), pl.ds(base, tile)] = value[: widths[g]]
+        return value[widths[g] :]
+
+    def convolve(which, i, g, gate):
+        of = pl.ds(channel[g], widths[g])
+        base = pl.multiple_of(bases[which] + i * tile, LANES)
+        near = conv_in[of, pl.ds(base, tile + LANES)]
+        total = jnp.zeros((widths[g], tile), f32)
         for k in range(TAPS):
-            start = PAD - TAPS + 1 + k
-            total = total + taps[k : k + 1] * near[start : start + tile]
+            moved = near if k == TAPS - 1 else pltpu.roll(near, TAPS - 1 - k, 1)
+            total = total + turned_taps[of, k : k + 1] * moved[:, LANES:]
         return gate * total
 
-    def split(half, at, value):
-        value = value.astype(bf16).astype(f32)
-        conv_in[half][pl.ds(at + PAD, tile), :] = value[:, :LANES]
-        return value[:, LANES:]
-
-    def convolution(half, product):
-        def own_product(i):
-            gates[pl.ds(i * tile, tile), :] = split(half, seq(own_base, i), product(0, i))
-
-        own_product(tiles - 1)
+    def own_product(i, g, at):
+        gates[pl.ds(channel[g], widths[g]), tile_at(i)] = product(OWN, i, g, at)
+
+    def own_last(g, at):
+        own_product(last, g, at)
+        of = pl.ds(channel[g], widths[g])
 
         @pl.when(me == 1)
         def _():
-            conv_in[half][pl.ds(0, PAD), :] = jnp.zeros((PAD, LANES), f32)
-            halo(conv_in[half], 2 * rows, PAD, 1 + half).start()
-
-        cols = pl.ds(half * LANES, LANES)
+            conv_in[of, pl.ds(0, LANES)] = jnp.zeros((widths[g], LANES), f32)
+            edge = jnp.transpose(conv_in[of, pl.ds(2 * rows, LANES)])
+            edge_out[g, :, pl.ds(0, widths[g])] = edge[LANES - PAD :]
+            edge_copy(g).start()
+
+    def mate_tiles(g, at):
+        of = pl.ds(channel[g], widths[g])
         for i in range(tiles):
-            at = seq(mate_base, i)
-            gate = split(half, at, product(1, i))
-            conv_out[pl.ds(i * tile, tile), cols] = convolve(half, at, gate).astype(bf16)
-            out_copy(half, i).start()
-        for i in range(tiles - 1):
-            own_product(i)
+            conv_out[of, tile_at(i)] = convolve(MATE, i, g, product(MATE, i, g, at)).astype(bf16)
+            out_copy(g, i).start()
+
+    def own_tiles(g, at):
+        of = pl.ds(channel[g], widths[g])
+
+        @pl.loop(0, last)
+        def _(i):
+            own_product(i, g, at)
 
         @pl.when(me == 2)
         def _():
-            halo(conv_in[half], 2 * rows, PAD, 1 + half).wait_recv()
-
-        for i in range(tiles):
-            at = pl.ds(i * tile, tile)
-            convolved = convolve(half, seq(own_base, i), gates[at, :])
-            mixed_ref[at, cols] = (attended[at, cols] + convolved).astype(bf16)
-
-    sources = (normed, other)
+            edge_copy(g).wait_recv()
+            edge = edge_in[g, :, pl.ds(0, widths[g])]
+            edge = jnp.concatenate([jnp.zeros((LANES - PAD, widths[g]), f32), edge], axis=0)
+            conv_in[of, pl.ds(0, LANES)] = jnp.transpose(edge)
+
+        @pl.loop(0, tiles)
+        def _(i):
+            convolved[of, tile_at(i)] = convolve(OWN, i, g, gates[of, tile_at(i)])
+
+    everything = pl.ds(0, conv_w.shape[1])
+
+    def mix(half, source):
+        cols = pl.ds(half * LANES, LANES)
+
+        @pl.loop(0, rows // LANES)
+        def _(i):
+            at = pl.ds(pl.multiple_of(i * LANES, LANES), LANES)
+            extra = jnp.transpose(source[cols, at].astype(f32))
+            mixed_ref[at, cols] = (attended[at, cols] + extra).astype(bf16)
 
     @pl.when(middle)
     def _():
-        for u in (CI0, CG0, CI1, CG1):
-            own_copies[u].wait()
-        forward_conv(CI1)
-        for shard in (peer, far):
-            for u in (CI0, CG0):
-                arrived(u, shard)
-        forward_conv(CG1)
+        forward_rest()
+        for u in (G0, G0_GATE):
+            arrived(u, peer)
+            arrived(u, far)
+        forward_conv(G2)
+        forward_conv(G3)
         relay(6)
         relay(7)
         for part in (fs * 2 + twin, across * 2 + twin, along * 2 + twin, diagonal * 2 + twin):
             for h in range(2):
                 piece_arrived(part, h)
 
-        def whole(which, i):
-            at = pl.ds(i * tile, tile)
-            return jnp.dot(sources[which][at, :], conv_w0[...], preferred_element_type=f32)
-
-        convolution(0, whole)
-        for u in (CI1, CG1):
-            arrived(u, peer)
-        for which in range(2):
-
-            @pl.loop(0, tiles)
-            def _(i):
-                at = pl.ds(pl.multiple_of(i * tile, tile), tile)
-                sums[which, at, :] = jnp.dot(
-                    sources[which][at, early], conv_w1[early, :], preferred_element_type=f32
-                )
-
-        for u in (CI1, CG1):
-            arrived(u, far)
-
-        def finish(which, i):
-            at = pl.ds(i * tile, tile)
-            return sums[which, at, :] + jnp.dot(
-                sources[which][at, late], conv_w1[late, :], preferred_element_type=f32
-            )
-
-        convolution(1, finish)
+        own_last(0, everything)
+        mate_tiles(0, everything)
+        partial(OWN, last, 1, pair, True)
+
+        @pl.loop(0, tiles)
+        def _(i):
+            partial(MATE, i, 1, pair, True)
+
+        arrived(G1, peer)
+        arrived(G1, far)
+        own_last(1, rest)
+        mate_tiles(1, rest)
+        own_tiles(0, everything)
+
+        @pl.loop(0, last)
+        def _(i):
+            partial(OWN, i, 1, pair, True)
+
+        arrived(G2, peer)
+        arrived(G3, peer)
+        partial(OWN, last, 2, shard_at(peer), False)
+
+        @pl.loop(0, tiles)
+        def _(i):
+            partial(MATE, i, 2, shard_at(peer), False)
+
+        for g in (2, 3):
+            arrived(G0_GATE + g, far)
+            own_last(g, shard_at(far))
+            mate_tiles(g, shard_at(far))
+        own_tiles(1, rest)
+
+        @pl.loop(0, last)
+        def _(i):
+            partial(OWN, i, 2, shard_at(peer), False)
+
+        for g in (2, 3):
+            own_tiles(g, shard_at(far))
+        for half in range(2):
+            mix(half, convolved)
 
     @pl.when(end)
     def _():
-        for half in range(2):
+        for i in range(tiles):
+            out_copy(0, i).wait_recv()
+        mix(0, conv_back)
+        for g in groups[1:]:
             for i in range(tiles):
-                at = (pl.ds(i * tile, tile), pl.ds(half * LANES, LANES))
-                out_copy(half, i).wait_recv()
-                mixed_ref[at] = (attended[at] + conv_back[at].astype(f32)).astype(bf16)
+                out_copy(g, i).wait_recv()
+        mix(1, conv_back)
 
     @pl.when(has_right)
     def _():
         kv_halo.wait_send()
 
     for u in (K, V, Q):
-        hop(u, me, True, True).wait_send()
+        hop(u, me, True).wait_send()
 
     @pl.when(end)
     def _():
         for h in range(2):
             piece_copy(normed, own_part, h, h, sp=mate).wait_send()
-        for u in (CI0, CG0, CI1, CG1):
-            hop(u, me, True, True).wait_send()
+        for u in units[G0:]:
+            hop(u, me, True).wait_send()
 
     @pl.when(middle)
     def _():
         for u in (K, V, Q):
             hop(u, peer, True).wait_send()
             hop(u, far, True).wait_send()
-        for u in range(7):
-            hop(u, me, False, True).wait_send()
+        for u in units:
+            hop(u, me, False).wait_send()
             hop(u, mate, False).wait_send()
         for j in range(len(relays)):
             for copy in relay_copies(j):
                 copy.wait_send()
-        for half in range(2):
+        for g in groups:
             for i in range(tiles):
-                out_copy(half, i).wait_send()
+                out_copy(g, i).wait_send()
 
         @pl.when(me == 1)
         def _():
-            for half in range(2):
-                halo(conv_in[half], 2 * rows, PAD, 1 + half).wait_send()
+            for g in groups:
+                edge_copy(g).wait_send()
 
 
 def paired_body(tokens, norm_gain, w_query, w_key, w_value, w_conv_in, w_conv_gate, conv_taps, sink_logits):
@@ -817,29 +896,32 @@
             pltpu.VMEM((rows, features), bf16),
             pltpu.VMEM((2 * HEAD_DIM, features), bf16),
             pltpu.VMEM((features, width), bf16),
-            pltpu.VMEM((features, width), bf16),
-            pltpu.VMEM((features, width), bf16),
+            pltpu.VMEM((2, w_query.shape[0], width), bf16),
+            pltpu.VMEM((2 * width, features), bf16),
             pltpu.VMEM((rows + WINDOW, 2 * HEAD_DIM), bf16),
             pltpu.VMEM((rows, width), bf16),
             pltpu.VMEM((rows, width), f32),
             pltpu.VMEM((rows, width), f32),
-            pltpu.VMEM((2 * rows + PAD, LANES), f32),
-            pltpu.VMEM((2 * rows + PAD, LANES), f32),
-            pltpu.VMEM((rows, LANES), f32),
-            pltpu.VMEM((2, rows, width), f32),
-            pltpu.VMEM((rows, width), bf16),
-            pltpu.VMEM((rows, width), bf16),
+            pltpu.VMEM((width, LANES + 2 * rows), f32),
+            pltpu.VMEM((width, rows), f32),
+            pltpu.VMEM((width, rows), f32),
+            pltpu.VMEM((2, width, rows), f32),
+            pltpu.VMEM((width, rows), bf16),
+            pltpu.VMEM((width, rows), bf16),
+            pltpu.VMEM((width, 8), f32),
+            pltpu.VMEM((4, PAD, LANES), f32),
+            pltpu.VMEM((4, PAD, LANES), f32),
             dma((8,)),
-            dma((7,)),
-            dma((7, 4)),
-            dma((7, 4)),
-            dma((7, 4)),
-            dma((3,)),
-            dma((3,)),
+            dma((5,)),
+            dma((8, 4)),
+            dma((8, 4)),
+            dma((8, 4)),
+            dma((5,)),
+            dma((5,)),
             dma((14,)),
             dma((16,)),
-            dma((2 * tiles,)),
-            dma((2 * tiles,)),
+            dma((4 * tiles,)),
+            dma((4 * tiles,)),
         ],
         compiler_params=pltpu.CompilerParams(
             collective_id=0, has_side_effects=True, vmem_limit_bytes=59 << 20

time: 60.8 us -> 68.5 us (1.13)
  the two profiles are of different devices: /device:TPU:0 before, /device:TPU:17 now
where the time goes in v2:
time: 68.5 us; the launch traced here: 68.3 us
  Pallas kernels  66.3 us (97%)
  local copies, waits for them, and re-layouts  1.4 us (2%)
    pallas_call x1, Pallas kernels, paired_body(): pl.pallas_call(paired_kernel, out_shape=(pltpu.VMEM((rows, width), bf16),...  66.3 us
    unnamed x2, local copies, waits for them, and re-layouts  1.4 us

profile of v2, /device:TPU:17, one launch (start us, length us, event | category | flops | bytes accessed | tf_op | source)
XLA Modules:
  0.0 68.3 jit_solution(262287217157227125)
XLA Ops:
  0.6 66.3 %paired_attend_convolve.1 = (bf16[1024,256]{1,0:T(8,128)(2,1)S(1)}, f32[4,1024]{1,0:T(4,128)S(1)}) custom-call(bf16[1024,2048]{1,0:T(8,128)(2,1)} %tok_ref.1, f32[1,2048]{1,0:T(1,128)} %bitcast.5, bf16[64,512]{1,0:T(8,128)(2,1)} %bitcast.3, bf16[64,512]{1,0:T(8,128)(2,1)} %bitcast.4, bf16[512,256]{1,0:T(8,128)(2,1)} %refs_2_.1, bf16[512,256]{1,0:T(8,128)(2,1)} %refs_3_.1, ...), custom_call_target="tpu_custom_call" | custom-call | tf_op jit(solution)/shard_map/paired_attend_convolve/pallas_call | solution.py:885
  66.9 0.8 %copy.13 = bf16[1024,256]{1,0:T(8,128)(2,1)} copy(bf16[1024,256]{1,0:T(8,128)(2,1)S(1)} %get-tuple-element.2) | data formatting | bytes 1048576
  67.7 0.6 copy.14

commit v3 on v2

--- a/solution.py
+++ b/solution.py
@@ -1,4 +1,5 @@
 import functools
+import math
 
 import jax
 import jax.numpy as jnp
@@ -13,6 +14,8 @@
 EPS = 1e-06
 LANES = 128
 PAD = 8
+LOG2_E = math.log2(math.e)
+LN_2 = math.log(2)
 MESH = pl.DeviceIdType.MESH
 
 
@@ -319,7 +322,7 @@
     (
         taps_ref, sink_ref, mixed_ref, log_ref,
         tok, normed, other, kv_all, q_all, stage, conv_w, kv, query, q_part, attended,
-        conv_in, gates, convolved, sums, conv_out, conv_back, turned_taps, edge_out, edge_in,
+        conv_in, convolved, sums, conv_out, conv_back, turned_taps, edge_out, edge_in,
         tok_sem, own_sem, recv_sem, mate_sem, peer_sem, halo_send, halo_recv,
         x_send, x_recv, out_send, out_recv,
     ) = refs[5:]
@@ -341,17 +344,15 @@
     depth = shards[2].shape[0]
     blocks = rows // WINDOW
     width = q_all.shape[1]
-    widths = (width // 2, width // 4, width // 8, width // 8)
+    widths = (width // 4, width // 4, width // 4, width // 8, width // 8)
     groups = range(len(widths))
     channel = [sum(widths[:g]) for g in groups]
-    K, V, Q, G0, G0_GATE, G1, G2, G3 = units = range(8)
-    spans = {G0: (0, width // 2), G0_GATE: (width // 2, width // 2)}
-    spans.update({G0_GATE + g: (2 * channel[g], 2 * widths[g]) for g in groups[1:]})
-    units_of = ((G0, G0_GATE), (G1,), (G2,), (G3,))
+    K, V, Q, A, B, C, D, E = units = range(8)
 
     parts = 8
     part_rows = rows // parts
-    piece = part_rows // 2
+    pieces = 4
+    piece = part_rows // pieces
     own_part = fs * 2 + tp
 
     def part_at(i):
@@ -376,13 +377,24 @@
             return kv_all.at[pl.ds(u * HEAD_DIM, HEAD_DIM), at]
         if u == Q:
             return q_all.at[at]
-        return conv_w.at[pl.ds(*spans[u]), at]
+        return conv_w.at[pl.ds(2 * channel[u - A], 2 * widths[u - A]), at]
 
     own_copies = [pltpu.make_async_copy(shards[u], place(u, me), own_sem.at[u]) for u in (K, V, Q)]
     own_copies += [pltpu.make_async_copy(shards[3 + j], stage.at[j], own_sem.at[3 + j]) for j in range(2)]
     for copy in own_copies:
         copy.start()
 
+    def norm_part(i):
+        tok_copies[i].wait()
+        norm_rows = 64
+
+        @pl.loop(0, part_rows // norm_rows)
+        def _(j):
+            at = rows_of(part_at(i) * part_rows + j * norm_rows, norm_rows)
+            wide = tok[at, :].astype(f32)
+            scale = lax.rsqrt(jnp.mean(wide * wide, axis=-1, keepdims=True) + EPS)
+            normed[at, :] = (wide * scale * gain_ref[...]).astype(bf16)
+
     barrier = pltpu.get_barrier_semaphore()
 
     def greet(**device):
@@ -397,6 +409,7 @@
         greet(fs=along)
         greet(tp=twin)
 
+    norm_part(0)
     own_copies[3].wait()
     own_copies[4].wait()
     for j in range(2):
@@ -426,25 +439,6 @@
     def arrived(u, shard):
         hop(u, shard, True).wait_recv()
 
-    for u in (K, V, Q):
-        hop(u, me, True).start()
-
-    @pl.when(middle)
-    def _():
-        for u in (K, V, Q):
-            hop(u, me, False).start()
-
-    def norm_part(i):
-        tok_copies[i].wait()
-        norm_rows = 64
-
-        @pl.loop(0, part_rows // norm_rows)
-        def _(j):
-            at = rows_of(part_at(i) * part_rows + j * norm_rows, norm_rows)
-            wide = tok[at, :].astype(f32)
-            scale = lax.rsqrt(jnp.mean(wide * wide, axis=-1, keepdims=True) + EPS)
-            normed[at, :] = (wide * scale * gain_ref[...]).astype(bf16)
-
     def piece_at(part, h):
         return rows_of(part * part_rows + h * piece, piece)
 
@@ -454,7 +448,7 @@
             src_ref=buffer.at[at],
             dst_ref=other.at[at],
             send_sem=x_send.at[i],
-            recv_sem=x_recv.at[part * 2 + h],
+            recv_sem=x_recv.at[part * pieces + h],
             device_id=device,
             device_id_type=MESH,
         )
@@ -463,16 +457,11 @@
         piece_copy(other, part, h, 0, sp=mate).wait_recv()
 
     across_part, along_part, diagonal_part = across * 2 + tp, along * 2 + tp, diagonal * 2 + tp
-    relays = (
-        (own_part, 0, ("tp", "fs_across", "fs_along")),
-        (own_part, 1, ("tp", "fs_across", "fs_along")),
-        (across_part, 0, ("tp", "fs_along")),
-        (along_part, 0, ("tp",)),
-        (across_part, 1, ("tp",)),
-        (along_part, 1, ("tp", "fs_across")),
-        (diagonal_part, 0, ("tp",)),
-        (diagonal_part, 1, ("tp",)),
-    )
+    relays = [(own_part, h, ("tp", "fs_across", "fs_along")) for h in range(pieces)]
+    relays += [(across_part, h, ("tp", "fs_along")[: 2 - h % 2]) for h in range(pieces)]
+    relays += [(along_part, h, ("tp", "fs_across")[: 1 + h % 2]) for h in range(pieces)]
+    relays += [(diagonal_part, h, ("tp",)) for h in range(pieces)]
+    OWN_X, ACROSS, ALONG, DIAGONAL = (pieces * j for j in range(4))
     devices = {"tp": {"tp": twin}, "fs_across": {"fs": across}, "fs_along": {"fs": along}}
 
     def relay_copies(j):
@@ -480,59 +469,61 @@
         part, h, to = relays[j]
         return [piece_copy(other, part, h, base + i, **devices[d]) for i, d in enumerate(to)]
 
-    def relay(j):
-        piece_arrived(relays[j][0], relays[j][1])
-        for copy in relay_copies(j):
-            copy.start()
-
-    norm_part(0)
-    norm_part(1)
+    def relay(*which):
+        for j in which:
+            piece_arrived(relays[j][0], relays[j][1])
+            for copy in relay_copies(j):
+                copy.start()
+
+    def send(to_mate, shard, *which):
+        for u in which:
+            hop(u, shard, to_mate).start()
+
+    def forward(to_mate, shard, *which):
+        for u in which:
+            arrived(u, shard)
+            hop(u, shard, to_mate).start()
+
+    def pieces_out(*which):
+        for h in which:
+            piece_copy(normed, own_part, h, h, sp=mate).start()
 
     @pl.when(end)
     def _():
-        for h in range(2):
-            piece_copy(normed, own_part, h, h, sp=mate).start()
-        for u in units[G0:]:
-            hop(u, me, True).start()
-
-    for i in range(2, parts):
+        pieces_out(0, 1)
+        send(True, me, K, V, Q)
+        pieces_out(2, 3)
+        send(True, me, A, B, C, D, E)
+
+    @pl.when(middle)
+    def _():
+        send(False, me, K, V, Q, A)
+        send(True, me, K, V, Q)
+
+    for i in range(1, parts):
         norm_part(i)
 
-    for u in (K, V):
-        arrived(u, mate)
-
-        @pl.when(middle)
-        def _():
-            hop(u, mate, False).start()
-
-        arrived(u, peer)
-
-        @pl.when(middle)
-        def _():
-            hop(u, peer, True).start()
-
-    arrived(Q, mate)
-
     @pl.when(middle)
     def _():
-        hop(Q, mate, False).start()
-        for u in (G0, G0_GATE, G1):
-            hop(u, me, False).start()
-
-    arrived(Q, peer)
-
-    @pl.when(middle)
-    def _():
-        hop(Q, peer, True).start()
-
-    for u in (K, V):
-        arrived(u, far)
-
-        @pl.when(middle)
-        def _():
-            hop(u, far, True).start()
-
-    tile = 256
+        relay(OWN_X)
+        forward(True, peer, K, V)
+        relay(OWN_X + 1, ACROSS, ALONG)
+        forward(False, mate, K, V)
+        send(False, me, B)
+        forward(True, peer, Q)
+        relay(ACROSS + 1, ALONG + 1)
+        forward(True, far, K)
+        forward(False, mate, Q)
+        send(False, me, C)
+        forward(True, far, V)
+
+    @pl.when(end)
+    def _():
+        for shard in (mate, peer, far):
+            for u in (K, V):
+                arrived(u, shard)
+
+    tile = 512
 
     @pl.loop(0, rows // tile)
     def _(i):
@@ -557,6 +548,15 @@
     def _():
         kv[pl.ds(0, WINDOW), :] = jnp.zeros((WINDOW, kv.shape[1]), bf16)
 
+    @pl.when(middle)
+    def _():
+        relay(DIAGONAL, DIAGONAL + 1)
+
+    @pl.when(end)
+    def _():
+        arrived(Q, mate)
+        arrived(Q, peer)
+
     early = pl.ds(pl.multiple_of(first * depth, depth), 3 * depth)
     late = pl.ds(pl.multiple_of(far * depth, depth), depth)
 
@@ -571,13 +571,13 @@
 
     @pl.when(middle)
     def _():
-        relay(0)
-
-    arrived(Q, far)
-
-    @pl.when(middle)
-    def _():
-        hop(Q, far, True).start()
+        relay(OWN_X + 2, OWN_X + 3, ACROSS + 2, ALONG + 2)
+        forward(True, far, Q)
+        forward(False, mate, A)
+
+    @pl.when(end)
+    def _():
+        arrived(Q, far)
 
     @pl.loop(0, rows // tile)
     def _(i):
@@ -591,71 +591,72 @@
     key_idx = lax.broadcasted_iota(jnp.int32, (WINDOW, 2 * WINDOW), 1)
     gap = query_idx + WINDOW - key_idx
     band = (gap >= 0) & (gap < WINDOW)
-    lane = lax.broadcasted_iota(jnp.int32, (2 * WINDOW, LANES), 1)
-    low_lanes = lane < HEAD_DIM
-    stat_lane = lax.broadcasted_iota(jnp.int32, (WINDOW, LANES), 1)
+    low_lanes = lax.broadcasted_iota(jnp.int32, (2 * WINDOW, LANES), 1) < HEAD_DIM
+    lane = lax.broadcasted_iota(jnp.int32, (WINDOW, LANES), 1)
+    low_half = lane < HEAD_DIM
 
     def attend(b, kept):
         base = pl.multiple_of(b * WINDOW, WINDOW)
         both = kv[pl.ds(base, 2 * WINDOW), :].astype(f32)
         turned = pltpu.roll(both, HEAD_DIM, 1)
-        zero = jnp.zeros_like(both)
-        keys = (jnp.where(low_lanes, both, zero).astype(bf16), jnp.where(low_lanes, zero, turned).astype(bf16))
-        vals = (jnp.where(low_lanes, turned, zero).astype(bf16), jnp.where(low_lanes, zero, both).astype(bf16))
-        stats = jnp.zeros((WINDOW, LANES), f32)
+        zero, one = jnp.zeros_like(both), jnp.ones_like(both)
+
+        def lower(x):
+            return jnp.where(low_lanes, x, zero)
+
+        def upper(x):
+            return jnp.where(low_lanes, zero, x)
+
+        keys = jnp.concatenate([lower(both), upper(turned)], axis=0).astype(bf16)
+        vals = jnp.concatenate([lower(turned), upper(both)], axis=0)
+        ones = jnp.concatenate([lower(one), upper(one)], axis=0)
+        vals = jnp.concatenate([vals, ones], axis=1).astype(bf16)
+        stats = []
         for pair in range(heads // 2):
             cols = pl.ds(pair * LANES, LANES)
-            q = query[pl.ds(base, WINDOW), cols]
-            out = None
+            scores = lax.dot_general(
+                query[pl.ds(base, WINDOW), cols], keys, (((1,), (1,)), ((), ())), preferred_element_type=f32
+            )
+            sinks = [sink_ref[2 * pair + side] * LOG2_E for side in range(2)]
+            tops, raised = [], []
             for side in range(2):
+                part = scores[:, side * 2 * WINDOW : (side + 1) * 2 * WINDOW] * (HEAD_DIM ** (-0.5) * LOG2_E)
+                part = jnp.where(kept, part, -jnp.inf)
+                tops.append(jnp.maximum(jnp.max(part, axis=-1, keepdims=True), sinks[side]))
+                raised.append(jnp.exp2(part - tops[side]).astype(bf16))
+            out = jnp.dot(jnp.concatenate(raised, axis=1), vals, preferred_element_type=f32)
+            top = jnp.where(low_half, tops[0], tops[1])
+            total = out[:, LANES:] + jnp.exp2(jnp.where(low_half, sinks[0], sinks[1]) - top)
+            attended[pl.ds(base, WINDOW), cols] = out[:, :LANES] / total
+            stats.append(top * LN_2 + jnp.log(total))
+        turned_stats = jnp.transpose(jnp.where(lax.rem(lane, 2) == 0, stats[0], stats[1]))
+        for pair in range(2):
+            for side in range(2):
+                row = pair + side * HEAD_DIM
                 head = 2 * pair + side
-                scores = lax.dot_general(
-                    q, keys[side], (((1,), (1,)), ((), ())), preferred_element_type=f32
-                ) * HEAD_DIM ** (-0.5)
-                scores = jnp.where(kept, scores, -jnp.inf)
-                sink = jnp.full((WINDOW, 1), sink_ref[head], f32)
-                top = jnp.maximum(jnp.max(scores, axis=-1, keepdims=True), sink)
-                raised = jnp.exp(scores - top)
-                total = jnp.sum(raised, axis=-1, keepdims=True) + jnp.exp(sink - top)
-                weights = (raised * (1.0 / total)).astype(bf16)
-                part = jnp.dot(weights, vals[side], preferred_element_type=f32)
-                out = part if out is None else out + part
-                stats = jnp.where(stat_lane == head, top + jnp.log(total), stats)
-            attended[pl.ds(base, WINDOW), cols] = out
-        log_ref[:, pl.ds(base, WINDOW)] = jnp.transpose(stats)[:heads]
-
-    def forward_conv(u):
-        arrived(u, mate)
-        hop(u, mate, False).start()
-
-    def forward_rest():
-        forward_conv(G1)
-        hop(G2, me, False).start()
-        hop(G3, me, False).start()
+                log_ref[head : head + 1, pl.ds(base, WINDOW)] = turned_stats[row : row + 1]
 
     services = (
-        (lambda: relay(1),),
-        (lambda: relay(2), lambda: relay(3)),
-        (lambda: forward_conv(G0),),
-        (lambda: forward_conv(G0_GATE),),
-        (lambda: relay(4), lambda: relay(5)),
+        lambda: relay(ACROSS + 3, ALONG + 3),
+        lambda: forward(False, mate, B),
+        lambda: relay(DIAGONAL + 2),
     )
-    cuts = [1 + (blocks - 1) * i // len(services) for i in range(len(services) + 1)]
-    for i, jobs in enumerate(services):
-
-        @pl.loop(cuts[i], cuts[i + 1])
-        def _(b):
-            attend(b, band)
+    for i, job in enumerate(services):
+
+        @pl.loop(i * (blocks // 2 - 1) // 3, (i + 1) * (blocks // 2 - 1) // 3)
+        def _(j):
+            attend(2 * j + 1, band)
+            attend(2 * j + 2, band)
 
         @pl.when(middle)
         def _():
-            for job in jobs:
-                job()
+            job()
 
     @pl.when(has_left)
     def _():
         kv_halo.wait_recv()
 
+    attend(blocks - 1, band)
     attend(0, band & ((key_idx >= WINDOW) | has_left))
 
     own_base, mate_base = jnp.where(me == 1, rows, 0), jnp.where(me == 1, 0, rows)
@@ -664,9 +665,6 @@
     tiles = rows // tile
     OWN, MATE = 0, 1
     last = tiles - 1
-    pair = pl.ds(pl.multiple_of(jnp.minimum(me, mate) * depth, depth), 2 * depth)
-    rest = pl.ds(pl.multiple_of(jnp.minimum(peer, far) * depth, depth), 2 * depth)
-
     def tile_at(i):
         return pl.ds(i * tile if isinstance(i, int) else pl.multiple_of(i * tile, tile), tile)
 
@@ -691,45 +689,41 @@
             device_id_type=MESH,
         )
 
-    def dot(which, i, start, length, at):
+    everything = pl.ds(0, conv_w.shape[1])
+
+    def dot(which, tokens, start, length, at):
         return lax.dot_general(
             conv_w[pl.ds(start, length), at],
-            sources[which][tile_at(i), at],
+            sources[which][tokens, at],
             (((1,), (1,)), ((), ())),
             preferred_element_type=f32,
         )
 
-    def partial(which, i, g, at, fresh):
-        start = 2 * channel[g]
-        value = dot(which, i, start, 2 * width - start, at)
-        to = pl.ds(start - 2 * widths[0], 2 * width - start)
-        sums[which, to, tile_at(i)] = value if fresh else sums[which, to, tile_at(i)] + value
-
-    def product(which, i, g, at):
-        value = dot(which, i, 2 * channel[g], 2 * widths[g], at)
-        if g:
-            value = value + sums[which, pl.ds(2 * channel[g] - 2 * widths[0], 2 * widths[g]), tile_at(i)]
+    small = 3
+    small_start = 2 * channel[small]
+    small_rows = 2 * width - small_start
+
+    def partial(which, i):
+        sums[which, :, tile_at(i)] = dot(which, tile_at(i), small_start, small_rows, early)
+
+    def keep(g, at, value):
         value = value.astype(bf16).astype(f32)
-        base = pl.multiple_of(bases[which] + LANES + i * tile, LANES)
-        conv_in[pl.ds(channel[g], widths[g]), pl.ds(base, tile)] = value[: widths[g]]
+        conv_in[pl.ds(channel[g], widths[g]), pl.ds(pl.multiple_of(at + LANES, LANES), value.shape[1])] = value[: widths[g]]
         return value[widths[g] :]
 
-    def convolve(which, i, g, gate):
+    def convolve(g, at, gate):
         of = pl.ds(channel[g], widths[g])
-        base = pl.multiple_of(bases[which] + i * tile, LANES)
-        near = conv_in[of, pl.ds(base, tile + LANES)]
+        near = conv_in[of, pl.ds(pl.multiple_of(at, LANES), tile + LANES)]
         total = jnp.zeros((widths[g], tile), f32)
         for k in range(TAPS):
             moved = near if k == TAPS - 1 else pltpu.roll(near, TAPS - 1 - k, 1)
             total = total + turned_taps[of, k : k + 1] * moved[:, LANES:]
         return gate * total
 
-    def own_product(i, g, at):
-        gates[pl.ds(channel[g], widths[g]), tile_at(i)] = product(OWN, i, g, at)
-
-    def own_last(g, at):
-        own_product(last, g, at)
+    def own_edge(g):
         of = pl.ds(channel[g], widths[g])
+        tokens = pl.ds(rows - LANES, LANES)
+        keep(g, own_base + rows - LANES, dot(OWN, tokens, 2 * channel[g], 2 * widths[g], everything))
 
         @pl.when(me == 1)
         def _():
@@ -738,31 +732,37 @@
             edge_out[g, :, pl.ds(0, widths[g])] = edge[LANES - PAD :]
             edge_copy(g).start()
 
-    def mate_tiles(g, at):
+    def mate_tiles(g):
         of = pl.ds(channel[g], widths[g])
         for i in range(tiles):
-            conv_out[of, tile_at(i)] = convolve(MATE, i, g, product(MATE, i, g, at)).astype(bf16)
+            at = mate_base + i * tile
+            if g < small:
+                value = dot(MATE, tile_at(i), 2 * channel[g], 2 * widths[g], everything)
+            else:
+                value = dot(MATE, tile_at(i), 2 * channel[g], 2 * widths[g], late)
+                value = value + sums[MATE, pl.ds(2 * channel[g] - small_start, 2 * widths[g]), tile_at(i)]
+            conv_out[of, tile_at(i)] = convolve(g, at, keep(g, at, value)).astype(bf16)
             out_copy(g, i).start()
 
-    def own_tiles(g, at):
-        of = pl.ds(channel[g], widths[g])
-
-        @pl.loop(0, last)
-        def _(i):
-            own_product(i, g, at)
-
+    def own_tiles(*which):
         @pl.when(me == 2)
         def _():
-            edge_copy(g).wait_recv()
-            edge = edge_in[g, :, pl.ds(0, widths[g])]
-            edge = jnp.concatenate([jnp.zeros((LANES - PAD, widths[g]), f32), edge], axis=0)
-            conv_in[of, pl.ds(0, LANES)] = jnp.transpose(edge)
-
-        @pl.loop(0, tiles)
-        def _(i):
-            convolved[of, tile_at(i)] = convolve(OWN, i, g, gates[of, tile_at(i)])
-
-    everything = pl.ds(0, conv_w.shape[1])
+            for g in which:
+                of = pl.ds(channel[g], widths[g])
+                edge_copy(g).wait_recv()
+                edge = edge_in[g, :, pl.ds(0, widths[g])]
+                edge = jnp.concatenate([jnp.zeros((LANES - PAD, widths[g]), f32), edge], axis=0)
+                conv_in[of, pl.ds(0, LANES)] = jnp.transpose(edge)
+
+        start = 2 * channel[which[0]]
+        length = sum(2 * widths[g] for g in which)
+        for i in range(tiles):
+            at = own_base + i * tile
+            value = dot(OWN, tile_at(i), start, length, everything)
+            for g in which:
+                row = 2 * channel[g] - start
+                gate = keep(g, at, value[row : row + 2 * widths[g]])
+                convolved[pl.ds(channel[g], widths[g]), tile_at(i)] = convolve(g, at, gate)
 
     def mix(half, source):
         cols = pl.ds(half * LANES, LANES)
@@ -775,68 +775,47 @@
 
     @pl.when(middle)
     def _():
-        forward_rest()
-        for u in (G0, G0_GATE):
-            arrived(u, peer)
-            arrived(u, far)
-        forward_conv(G2)
-        forward_conv(G3)
-        relay(6)
-        relay(7)
+        forward(False, mate, C)
+        send(False, me, D, E)
+        relay(DIAGONAL + 3)
         for part in (fs * 2 + twin, across * 2 + twin, along * 2 + twin, diagonal * 2 + twin):
-            for h in range(2):
+            for h in range(pieces):
                 piece_arrived(part, h)
 
-        own_last(0, everything)
-        mate_tiles(0, everything)
-        partial(OWN, last, 1, pair, True)
-
-        @pl.loop(0, tiles)
-        def _(i):
-            partial(MATE, i, 1, pair, True)
-
-        arrived(G1, peer)
-        arrived(G1, far)
-        own_last(1, rest)
-        mate_tiles(1, rest)
-        own_tiles(0, everything)
-
-        @pl.loop(0, last)
-        def _(i):
-            partial(OWN, i, 1, pair, True)
-
-        arrived(G2, peer)
-        arrived(G3, peer)
-        partial(OWN, last, 2, shard_at(peer), False)
-
-        @pl.loop(0, tiles)
-        def _(i):
-            partial(MATE, i, 2, shard_at(peer), False)
-
-        for g in (2, 3):
-            arrived(G0_GATE + g, far)
-            own_last(g, shard_at(far))
-            mate_tiles(g, shard_at(far))
-        own_tiles(1, rest)
-
-        @pl.loop(0, last)
-        def _(i):
-            partial(OWN, i, 2, shard_at(peer), False)
-
-        for g in (2, 3):
-            own_tiles(g, shard_at(far))
+        def ready(*which):
+            for u in which:
+                arrived(u, peer)
+                arrived(u, far)
+
+        for g in range(2):
+            ready(A + g)
+            own_edge(g)
+            mate_tiles(g)
+        forward(False, mate, D, E)
+        own_tiles(0, 1)
+        mix(0, convolved)
+        ready(C)
+        own_edge(2)
+        mate_tiles(2)
+        arrived(D, peer)
+        arrived(E, peer)
+        for i in range(tiles):
+            partial(MATE, i)
+        for g in (3, 4):
+            arrived(A + g, far)
+            own_edge(g)
+            mate_tiles(g)
+        own_tiles(2)
+        own_tiles(3, 4)
+        mix(1, convolved)
+
+    @pl.when(end)
+    def _():
         for half in range(2):
-            mix(half, convolved)
-
-    @pl.when(end)
-    def _():
-        for i in range(tiles):
-            out_copy(0, i).wait_recv()
-        mix(0, conv_back)
-        for g in groups[1:]:
-            for i in range(tiles):
-                out_copy(g, i).wait_recv()
-        mix(1, conv_back)
+            for g in (groups[:2], groups[2:])[half]:
+                for i in range(tiles):
+                    out_copy(g, i).wait_recv()
+            mix(half, conv_back)
 
     @pl.when(has_right)
     def _():
@@ -847,9 +826,9 @@
 
     @pl.when(end)
     def _():
-        for h in range(2):
+        for h in range(pieces):
             piece_copy(normed, own_part, h, h, sp=mate).wait_send()
-        for u in units[G0:]:
+        for u in units[A:]:
             hop(u, me, True).wait_send()
 
     @pl.when(middle)
@@ -881,7 +860,7 @@
     vmem = pl.BlockSpec(memory_space=pltpu.VMEM)
     smem = pl.BlockSpec(memory_space=pltpu.SMEM)
     dma = pltpu.SemaphoreType.DMA
-    tiles = rows // 256
+    tiles = rows // 512
     return pl.pallas_call(
         paired_kernel,
         out_shape=(
@@ -904,24 +883,23 @@
             pltpu.VMEM((rows, width), f32),
             pltpu.VMEM((width, LANES + 2 * rows), f32),
             pltpu.VMEM((width, rows), f32),
-            pltpu.VMEM((width, rows), f32),
-            pltpu.VMEM((2, width, rows), f32),
+            pltpu.VMEM((2, width // 2, rows), f32),
             pltpu.VMEM((width, rows), bf16),
             pltpu.VMEM((width, rows), bf16),
             pltpu.VMEM((width, 8), f32),
-            pltpu.VMEM((4, PAD, LANES), f32),
-            pltpu.VMEM((4, PAD, LANES), f32),
+            pltpu.VMEM((5, PAD, LANES), f32),
+            pltpu.VMEM((5, PAD, LANES), f32),
             dma((8,)),
             dma((5,)),
             dma((8, 4)),
             dma((8, 4)),
             dma((8, 4)),
-            dma((5,)),
-            dma((5,)),
-            dma((14,)),
-            dma((16,)),
-            dma((4 * tiles,)),
-            dma((4 * tiles,)),
+            dma((6,)),
+            dma((6,)),
+            dma((28,)),
+            dma((32,)),
+            dma((5 * tiles,)),
+            dma((5 * tiles,)),
         ],
         compiler_params=pltpu.CompilerParams(
             collective_id=0, has_side_effects=True, vmem_limit_bytes=59 << 20

time: 68.5 us -> 60.3 us (0.88)
  the two profiles are of different devices: /device:TPU:17 before, /device:TPU:0 now
where the time goes in v3:
time: 60.3 us; the launch traced here: 60 us
  Pallas kernels  57.9 us (96%)
  local copies, waits for them, and re-layouts  1.4 us (2%)
  between operations  0.64 us (1%)
    pallas_call x1, Pallas kernels, paired_body(): pl.pallas_call(paired_kernel, out_shape=(pltpu.VMEM((rows, width), bf16),...  57.9 us
    unnamed x2, local copies, waits for them, and re-layouts  1.4 us

profile of v3, /device:TPU:0, one launch (start us, length us, event | category | flops | bytes accessed | tf_op | source)
XLA Modules:
  0.0 60.0 jit_solution(2839411054505862312)
XLA Ops:
  0.6 57.9 %paired_attend_convolve.1 = (bf16[1024,256]{1,0:T(8,128)(2,1)S(1)}, f32[4,1024]{1,0:T(4,128)S(1)}) custom-call(bf16[1024,2048]{1,0:T(8,128)(2,1)} %tok_ref.1, f32[1,2048]{1,0:T(1,128)} %bitcast.5, bf16[64,512]{1,0:T(8,128)(2,1)} %bitcast.3, bf16[64,512]{1,0:T(8,128)(2,1)} %bitcast.4, bf16[512,256]{1,0:T(8,128)(2,1)} %refs_2_.1, bf16[512,256]{1,0:T(8,128)(2,1)} %refs_3_.1, ...), custom_call_target="tpu_custom_call" | custom-call | tf_op jit(solution)/shard_map/paired_attend_convolve/pallas_call | solution.py:864
  58.6 0.8 %copy.13 = bf16[1024,256]{1,0:T(8,128)(2,1)} copy(bf16[1024,256]{1,0:T(8,128)(2,1)S(1)} %get-tuple-element.2) | data formatting | bytes 1048576
  59.4 0.6 %copy.14 = f32[4,1024]{1,0:T(4,128)} copy(f32[4,1024]{1,0:T(4,128)S(1)} %get-tuple-element.3) | data formatting | bytes 32768

commit v4 on v3

--- a/solution.py
+++ b/solution.py
@@ -490,14 +490,12 @@
 
     @pl.when(end)
     def _():
-        pieces_out(0, 1)
-        send(True, me, K, V, Q)
-        pieces_out(2, 3)
-        send(True, me, A, B, C, D, E)
+        pieces_out(*range(pieces))
+        send(True, me, K, V, Q, A, B, C)
 
     @pl.when(middle)
     def _():
-        send(False, me, K, V, Q, A)
+        send(False, me, K, V, Q, A, B, C)
         send(True, me, K, V, Q)
 
     for i in range(1, parts):
@@ -508,14 +506,12 @@
         relay(OWN_X)
         forward(True, peer, K, V)
         relay(OWN_X + 1, ACROSS, ALONG)
+        forward(True, peer, Q)
+        relay(OWN_X + 2, ACROSS + 1, ALONG + 1, OWN_X + 3, ACROSS + 2, ALONG + 2)
         forward(False, mate, K, V)
-        send(False, me, B)
-        forward(True, peer, Q)
-        relay(ACROSS + 1, ALONG + 1)
-        forward(True, far, K)
-        forward(False, mate, Q)
-        send(False, me, C)
-        forward(True, far, V)
+        send(False, me, D, E)
+        relay(ACROSS + 3, ALONG + 3, DIAGONAL, DIAGONAL + 1)
+        forward(True, far, K, V)
 
     @pl.when(end)
     def _():
@@ -548,12 +544,17 @@
     def _():
         kv[pl.ds(0, WINDOW), :] = jnp.zeros((WINDOW, kv.shape[1]), bf16)
 
+    @pl.when(has_right)
+    def _():
+        kv_halo.start()
+
     @pl.when(middle)
     def _():
-        relay(DIAGONAL, DIAGONAL + 1)
+        forward(False, mate, Q)
 
     @pl.when(end)
     def _():
+        send(True, me, D, E)
         arrived(Q, mate)
         arrived(Q, peer)
 
@@ -565,15 +566,133 @@
         at = pl.ds(pl.multiple_of(i * tile, tile), tile)
         q_part[at, :] = jnp.dot(normed[at, early], q_all[early, :], preferred_element_type=f32)
 
-    @pl.when(has_right)
-    def _():
-        kv_halo.start()
+    own_base, mate_base = jnp.where(me == 1, rows, 0), jnp.where(me == 1, 0, rows)
+    bases = (own_base, mate_base)
+    sources = (normed, other)
+    tiles = rows // tile
+    OWN, MATE = 0, 1
+    last = tiles - 1
+    def tile_at(i):
+        return pl.ds(i * tile if isinstance(i, int) else pl.multiple_of(i * tile, tile), tile)
+
+    def out_copy(g, i):
+        at = (pl.ds(channel[g], widths[g]), tile_at(i))
+        return pltpu.make_async_remote_copy(
+            src_ref=conv_out.at[at],
+            dst_ref=conv_back.at[at],
+            send_sem=out_send.at[g * tiles + i],
+            recv_sem=out_recv.at[g * tiles + i],
+            device_id={"sp": mate},
+            device_id_type=MESH,
+        )
+
+    def edge_copy(g):
+        return pltpu.make_async_remote_copy(
+            src_ref=edge_out.at[g],
+            dst_ref=edge_in.at[g],
+            send_sem=halo_send.at[1 + g],
+            recv_sem=halo_recv.at[1 + g],
+            device_id={"sp": right},
+            device_id_type=MESH,
+        )
+
+    center = pl.ds(depth, 2 * depth)
+
+    def dot(which, tokens, start, length, at):
+        return lax.dot_general(
+            conv_w[pl.ds(start, length), at],
+            sources[which][tokens, at],
+            (((1,), (1,)), ((), ())),
+            preferred_element_type=f32,
+        )
+
+    def partial(which, u, v, at, fresh):
+        start = 2 * channel[u - A]
+        span = pl.ds(start, 2 * channel[v - A] + 2 * widths[v - A] - start)
+        for i in range(tiles):
+            value = dot(which, tile_at(i), span.start, span.size, at)
+            sums[which, span, tile_at(i)] = value if fresh else sums[which, span, tile_at(i)] + value
+
+    def product(which, tokens, start, length):
+        return sums[which, pl.ds(start, length), tokens] + dot(which, tokens, start, length, late)
+
+    def keep(g, at, value):
+        value = value.astype(bf16).astype(f32)
+        conv_in[pl.ds(channel[g], widths[g]), pl.ds(pl.multiple_of(at + LANES, LANES), value.shape[1])] = value[: widths[g]]
+        return value[widths[g] :]
+
+    def convolve(g, at, gate):
+        of = pl.ds(channel[g], widths[g])
+        near = conv_in[of, pl.ds(pl.multiple_of(at, LANES), tile + LANES)]
+        total = jnp.zeros((widths[g], tile), f32)
+        for k in range(TAPS):
+            moved = near if k == TAPS - 1 else pltpu.roll(near, TAPS - 1 - k, 1)
+            total = total + turned_taps[of, k : k + 1] * moved[:, LANES:]
+        return gate * total
+
+    def own_edge(g):
+        of = pl.ds(channel[g], widths[g])
+        tokens = pl.ds(rows - LANES, LANES)
+        keep(g, own_base + rows - LANES, product(OWN, tokens, 2 * channel[g], 2 * widths[g]))
+
+        @pl.when(me == 1)
+        def _():
+            conv_in[of, pl.ds(0, LANES)] = jnp.zeros((widths[g], LANES), f32)
+            edge = jnp.transpose(conv_in[of, pl.ds(2 * rows, LANES)])
+            edge_out[g, :, pl.ds(0, widths[g])] = edge[LANES - PAD :]
+            edge_copy(g).start()
+
+    def mate_tiles(g):
+        of = pl.ds(channel[g], widths[g])
+        for i in range(tiles):
+            at = mate_base + i * tile
+            value = product(MATE, tile_at(i), 2 * channel[g], 2 * widths[g])
+            conv_out[of, tile_at(i)] = convolve(g, at, keep(g, at, value)).astype(bf16)
+            out_copy(g, i).start()
+
+    def own_tiles(*which):
+        @pl.when(me == 2)
+        def _():
+            for g in which:
+                of = pl.ds(channel[g], widths[g])
+                edge_copy(g).wait_recv()
+                edge = edge_in[g, :, pl.ds(0, widths[g])]
+                edge = jnp.concatenate([jnp.zeros((LANES - PAD, widths[g]), f32), edge], axis=0)
+                conv_in[of, pl.ds(0, LANES)] = jnp.transpose(edge)
+
+        start = 2 * channel[which[0]]
+        length = sum(2 * widths[g] for g in which)
+        for i in range(tiles):
+            at = own_base + i * tile
+            value = product(OWN, tile_at(i), start, length)
+            for g in which:
+                row = 2 * channel[g] - start
+                gate = keep(g, at, value[row : row + 2 * widths[g]])
+                convolved[pl.ds(channel[g], widths[g]), tile_at(i)] = convolve(g, at, gate)
+
+    def mix(half, i, source):
+        cols = pl.ds(half * LANES, LANES)
+        for j in range(tile // LANES):
+            at = pl.ds(i * tile + j * LANES, LANES)
+            extra = jnp.transpose(source[cols, at].astype(f32))
+            mixed_ref[at, cols] = (attended[at, cols] + extra).astype(bf16)
 
     @pl.when(middle)
     def _():
-        relay(OWN_X + 2, OWN_X + 3, ACROSS + 2, ALONG + 2)
+        relay(DIAGONAL + 2)
+        for u in units[A:]:
+            arrived(u, peer)
+        partial(OWN, A, E, center, True)
+        forward(False, mate, A)
+        relay(DIAGONAL + 3)
+        for part in (fs * 2 + twin, across * 2 + twin, along * 2 + twin, diagonal * 2 + twin):
+            for h in range(pieces):
+                piece_arrived(part, h)
+        partial(MATE, A, E, center, True)
+        forward(False, mate, B)
+        for which in (OWN, MATE):
+            partial(which, A, B, shard_at(mate), False)
         forward(True, far, Q)
-        forward(False, mate, A)
 
     @pl.when(end)
     def _():
@@ -637,9 +756,9 @@
                 log_ref[head : head + 1, pl.ds(base, WINDOW)] = turned_stats[row : row + 1]
 
     services = (
-        lambda: relay(ACROSS + 3, ALONG + 3),
-        lambda: forward(False, mate, B),
-        lambda: relay(DIAGONAL + 2),
+        lambda: forward(False, mate, C),
+        lambda: None,
+        lambda: forward(False, mate, D, E),
     )
     for i, job in enumerate(services):
 
@@ -659,163 +778,34 @@
     attend(blocks - 1, band)
     attend(0, band & ((key_idx >= WINDOW) | has_left))
 
-    own_base, mate_base = jnp.where(me == 1, rows, 0), jnp.where(me == 1, 0, rows)
-    bases = (own_base, mate_base)
-    sources = (normed, other)
-    tiles = rows // tile
-    OWN, MATE = 0, 1
-    last = tiles - 1
-    def tile_at(i):
-        return pl.ds(i * tile if isinstance(i, int) else pl.multiple_of(i * tile, tile), tile)
-
-    def out_copy(g, i):
-        at = (pl.ds(channel[g], widths[g]), tile_at(i))
-        return pltpu.make_async_remote_copy(
-            src_ref=conv_out.at[at],
-            dst_ref=conv_back.at[at],
-            send_sem=out_send.at[g * tiles + i],
-            recv_sem=out_recv.at[g * tiles + i],
-            device_id={"sp": mate},
-            device_id_type=MESH,
-        )
-
-    def edge_copy(g):
-        return pltpu.make_async_remote_copy(
-            src_ref=edge_out.at[g],
-            dst_ref=edge_in.at[g],
-            send_sem=halo_send.at[1 + g],
-            recv_sem=halo_recv.at[1 + g],
-            device_id={"sp": right},
-            device_id_type=MESH,
-        )
-
-    everything = pl.ds(0, conv_w.shape[1])
-
-    def dot(which, tokens, start, length, at):
-        return lax.dot_general(
-            conv_w[pl.ds(start, length), at],
-            sources[which][tokens, at],
-            (((1,), (1,)), ((), ())),
-            preferred_element_type=f32,
-        )
-
-    small = 3
-    small_start = 2 * channel[small]
-    small_rows = 2 * width - small_start
-
-    def partial(which, i):
-        sums[which, :, tile_at(i)] = dot(which, tile_at(i), small_start, small_rows, early)
-
-    def keep(g, at, value):
-        value = value.astype(bf16).astype(f32)
-        conv_in[pl.ds(channel[g], widths[g]), pl.ds(pl.multiple_of(at + LANES, LANES), value.shape[1])] = value[: widths[g]]
-        return value[widths[g] :]
-
-    def convolve(g, at, gate):
-        of = pl.ds(channel[g], widths[g])
-        near = conv_in[of, pl.ds(pl.multiple_of(at, LANES), tile + LANES)]
-        total = jnp.zeros((widths[g], tile), f32)
-        for k in range(TAPS):
-            moved = near if k == TAPS - 1 else pltpu.roll(near, TAPS - 1 - k, 1)
-            total = total + turned_taps[of, k : k + 1] * moved[:, LANES:]
-        return gate * total
-
-    def own_edge(g):
-        of = pl.ds(channel[g], widths[g])
-        tokens = pl.ds(rows - LANES, LANES)
-        keep(g, own_base + rows - LANES, dot(OWN, tokens, 2 * channel[g], 2 * widths[g], everything))
-
-        @pl.when(me == 1)
-        def _():
-            conv_in[of, pl.ds(0, LANES)] = jnp.zeros((widths[g], LANES), f32)
-            edge = jnp.transpose(conv_in[of, pl.ds(2 * rows, LANES)])
-            edge_out[g, :, pl.ds(0, widths[g])] = edge[LANES - PAD :]
-            edge_copy(g).start()
-
-    def mate_tiles(g):
-        of = pl.ds(channel[g], widths[g])
-        for i in range(tiles):
-            at = mate_base + i * tile
-            if g < small:
-                value = dot(MATE, tile_at(i), 2 * channel[g], 2 * widths[g], everything)
-            else:
-                value = dot(MATE, tile_at(i), 2 * channel[g], 2 * widths[g], late)
-                value = value + sums[MATE, pl.ds(2 * channel[g] - small_start, 2 * widths[g]), tile_at(i)]
-            conv_out[of, tile_at(i)] = convolve(g, at, keep(g, at, value)).astype(bf16)
-            out_copy(g, i).start()
-
-    def own_tiles(*which):
-        @pl.when(me == 2)
-        def _():
-            for g in which:
-                of = pl.ds(channel[g], widths[g])
-                edge_copy(g).wait_recv()
-                edge = edge_in[g, :, pl.ds(0, widths[g])]
-                edge = jnp.concatenate([jnp.zeros((LANES - PAD, widths[g]), f32), edge], axis=0)
-                conv_in[of, pl.ds(0, LANES)] = jnp.transpose(edge)
-
-        start = 2 * channel[which[0]]
-        length = sum(2 * widths[g] for g in which)
-        for i in range(tiles):
-            at = own_base + i * tile
-            value = dot(OWN, tile_at(i), start, length, everything)
-            for g in which:
-                row = 2 * channel[g] - start
-                gate = keep(g, at, value[row : row + 2 * widths[g]])
-                convolved[pl.ds(channel[g], widths[g]), tile_at(i)] = convolve(g, at, gate)
-
-    def mix(half, source):
-        cols = pl.ds(half * LANES, LANES)
-
-        @pl.loop(0, rows // LANES)
-        def _(i):
-            at = pl.ds(pl.multiple_of(i * LANES, LANES), LANES)
-            extra = jnp.transpose(source[cols, at].astype(f32))
-            mixed_ref[at, cols] = (attended[at, cols] + extra).astype(bf16)
-
     @pl.when(middle)
     def _():
-        forward(False, mate, C)
-        send(False, me, D, E)
-        relay(DIAGONAL + 3)
-        for part in (fs * 2 + twin, across * 2 + twin, along * 2 + twin, diagonal * 2 + twin):
-            for h in range(pieces):
-                piece_arrived(part, h)
-
-        def ready(*which):
-            for u in which:
-                arrived(u, peer)
-                arrived(u, far)
-
-        for g in range(2):
-            ready(A + g)
-            own_edge(g)
-            mate_tiles(g)
-        forward(False, mate, D, E)
-        own_tiles(0, 1)
-        mix(0, convolved)
-        ready(C)
-        own_edge(2)
-        mate_tiles(2)
-        arrived(D, peer)
-        arrived(E, peer)
-        for i in range(tiles):
-            partial(MATE, i)
-        for g in (3, 4):
+        def finish(g):
             arrived(A + g, far)
             own_edge(g)
             mate_tiles(g)
-        own_tiles(2)
-        own_tiles(3, 4)
-        mix(1, convolved)
+
+        finish(0)
+        for which in (MATE, OWN):
+            partial(which, C, E, shard_at(mate), False)
+        finish(1)
+        own_tiles(0, 1)
+        for i in range(tiles):
+            mix(0, i, convolved)
+        finish(2)
+        finish(3)
+        finish(4)
+        own_tiles(2, 3, 4)
+        for i in range(tiles):
+            mix(1, i, convolved)
 
     @pl.when(end)
     def _():
         for half in range(2):
-            for g in (groups[:2], groups[2:])[half]:
-                for i in range(tiles):
+            for i in range(tiles):
+                for g in (groups[:2], groups[2:])[half]:
                     out_copy(g, i).wait_recv()
-            mix(half, conv_back)
+                mix(half, i, conv_back)
 
     @pl.when(has_right)
     def _():
@@ -883,7 +873,7 @@
             pltpu.VMEM((rows, width), f32),
             pltpu.VMEM((width, LANES + 2 * rows), f32),
             pltpu.VMEM((width, rows), f32),
-            pltpu.VMEM((2, width // 2, rows), f32),
+            pltpu.VMEM((2, 2 * width, rows), f32),
             pltpu.VMEM((width, rows), bf16),
             pltpu.VMEM((width, rows), bf16),
             pltpu.VMEM((width, 8), f32),

time: 60.3 us -> 61 us (1.012)
  Pallas kernels: 57.9 us -> 58.8 us
    pallas_call x1, Pallas kernels: 57.9 us -> 58.8 us  [paired_body(): pl.pallas_call(paired_kernel, out_shape=(pltpu.VMEM((rows, width), bf16),...]
where the time goes in v4:
time: 61 us; the launch traced here: 60.8 us
  Pallas kernels  58.8 us (96%)
  local copies, waits for them, and re-layouts  1.4 us (2%)
  between operations  0.64 us (1%)
    pallas_call x1, Pallas kernels, paired_body(): pl.pallas_call(paired_kernel, out_shape=(pltpu.VMEM((rows, width), bf16),...  58.8 us
    unnamed x2, local copies, waits for them, and re-layouts  1.4 us

profile of v4, /device:TPU:0, one launch (start us, length us, event | category | flops | bytes accessed | tf_op | source)
XLA Modules:
  0.0 60.8 jit_solution(1743512998768598343)
XLA Ops:
  0.6 58.8 %paired_attend_convolve.1 = (bf16[1024,256]{1,0:T(8,128)(2,1)S(1)}, f32[4,1024]{1,0:T(4,128)S(1)}) custom-call(bf16[1024,2048]{1,0:T(8,128)(2,1)} %tok_ref.1, f32[1,2048]{1,0:T(1,128)} %bitcast.5, bf16[64,512]{1,0:T(8,128)(2,1)} %bitcast.3, bf16[64,512]{1,0:T(8,128)(2,1)} %bitcast.4, bf16[512,256]{1,0:T(8,128)(2,1)} %refs_2_.1, bf16[512,256]{1,0:T(8,128)(2,1)} %refs_3_.1, ...), custom_call_target="tpu_custom_call" | custom-call | tf_op jit(solution)/shard_map/paired_attend_convolve/pallas_call | solution.py:854
  59.4 0.8 %copy.13 = bf16[1024,256]{1,0:T(8,128)(2,1)} copy(bf16[1024,256]{1,0:T(8,128)(2,1)S(1)} %get-tuple-element.2) | data formatting | bytes 1048576
  60.2 0.6 copy.14

commit v5 on v4

--- a/solution.py
+++ b/solution.py
@@ -323,8 +323,7 @@
         taps_ref, sink_ref, mixed_ref, log_ref,
         tok, normed, other, kv_all, q_all, stage, conv_w, kv, query, q_part, attended,
         conv_in, convolved, sums, conv_out, conv_back, turned_taps, edge_out, edge_in,
-        tok_sem, own_sem, recv_sem, mate_sem, peer_sem, halo_send, halo_recv,
-        x_send, x_recv, out_send, out_recv,
+        tok_sem, own_sem, recv_sem, sent_sem, halo_recv, x_recv, twin_recv, out_recv,
     ) = refs[5:]
     f32, bf16 = jnp.float32, jnp.bfloat16
     me, fs, tp = lax.axis_index("sp"), lax.axis_index("fs"), lax.axis_index("tp")
@@ -347,7 +346,7 @@
     widths = (width // 4, width // 4, width // 4, width // 8, width // 8)
     groups = range(len(widths))
     channel = [sum(widths[:g]) for g in groups]
-    K, V, Q, A, B, C, D, E = units = range(8)
+    K, V, Q, R, A, B, C, D, E = units = range(9)
 
     parts = 8
     part_rows = rows // parts
@@ -364,7 +363,7 @@
     tok_copies = []
     for i in range(parts):
         at = rows_of(part_at(i) * part_rows, part_rows)
-        tok_copies.append(pltpu.make_async_copy(tok_ref.at[at], tok.at[at], tok_sem.at[i]))
+        tok_copies.append(pltpu.make_async_copy(tok_ref.at[at], tok.at[at], tok_sem.at[min(i, 1)]))
     for copy in tok_copies:
         copy.start()
 
@@ -375,17 +374,17 @@
         at = shard_at(shard)
         if u < Q:
             return kv_all.at[pl.ds(u * HEAD_DIM, HEAD_DIM), at]
-        if u == Q:
-            return q_all.at[at]
+        if u < A:
+            return q_all.at[at, pl.ds((u - Q) * LANES, LANES)]
         return conv_w.at[pl.ds(2 * channel[u - A], 2 * widths[u - A]), at]
 
-    own_copies = [pltpu.make_async_copy(shards[u], place(u, me), own_sem.at[u]) for u in (K, V, Q)]
-    own_copies += [pltpu.make_async_copy(shards[3 + j], stage.at[j], own_sem.at[3 + j]) for j in range(2)]
+    own_copies = [pltpu.make_async_copy(shards[u], place(u, me), own_sem.at[0]) for u in (K, V)]
+    own_copies.append(pltpu.make_async_copy(shards[2], q_all.at[shard_at(me)], own_sem.at[1]))
+    own_copies += [pltpu.make_async_copy(shards[3 + j], stage.at[j], own_sem.at[2]) for j in range(2)]
     for copy in own_copies:
         copy.start()
 
     def norm_part(i):
-        tok_copies[i].wait()
         norm_rows = 64
 
         @pl.loop(0, part_rows // norm_rows)
@@ -409,9 +408,9 @@
         greet(fs=along)
         greet(tp=twin)
 
+    tok_copies[0].wait()
     norm_part(0)
-    own_copies[3].wait()
-    own_copies[4].wait()
+    pltpu.make_async_copy(stage, stage, own_sem.at[2]).wait()
     for j in range(2):
         for block in range(depth // LANES):
             turned = jnp.transpose(stage[j, pl.ds(block * LANES, LANES), :].astype(f32)).astype(bf16)
@@ -421,40 +420,57 @@
                 conv_w[to, at] = turned[channel[g] : channel[g] + widths[g]]
     taps = taps_ref[...].astype(f32)
     turned_taps[...] = jnp.transpose(jnp.concatenate([taps, jnp.zeros((8 - TAPS, width), f32)], axis=0))
-    for u in (K, V, Q):
-        own_copies[u].wait()
+    own_kv = kv_all.at[:, shard_at(me)]
+    pltpu.make_async_copy(own_kv, own_kv, own_sem.at[0]).wait()
+    own_copies[2].wait()
+    conv_in[:, pl.ds(0, LANES)] = jnp.zeros((width, LANES), f32)
 
     pl.semaphore_wait(barrier, jnp.where(middle, 5, 1))
 
+    TO_MATE, TO_PEER, RELAYED, RETURNED, EDGES, HALO = range(6)
+
+    def slot(shard, device):
+        return shard - jnp.where(shard > device, 1, 0)
+
     def hop(u, shard, to_mate):
+        target = mate if to_mate else peer
         return pltpu.make_async_remote_copy(
             src_ref=place(u, shard),
             dst_ref=place(u, shard),
-            send_sem=(mate_sem if to_mate else peer_sem).at[u, shard],
-            recv_sem=recv_sem.at[u, shard],
-            device_id={"sp": mate if to_mate else peer},
+            send_sem=sent_sem.at[TO_MATE if to_mate else TO_PEER],
+            recv_sem=recv_sem.at[u, slot(shard, target)],
+            device_id={"sp": target},
             device_id_type=MESH,
         )
 
     def arrived(u, shard):
-        hop(u, shard, True).wait_recv()
+        ref = place(u, shard)
+        pltpu.make_async_copy(ref, ref, recv_sem.at[u, slot(shard, me)]).wait()
+
+    def drain(kind, elements):
+        ref = other.at[pl.ds(0, elements // other.shape[1])]
+        pltpu.make_async_copy(ref, ref, sent_sem.at[kind]).wait()
 
     def piece_at(part, h):
         return rows_of(part * part_rows + h * piece, piece)
 
-    def piece_copy(buffer, part, h, i, **device):
+    def piece_copy(buffer, part, h, kind, arrival, **device):
         at = piece_at(part, h)
         return pltpu.make_async_remote_copy(
             src_ref=buffer.at[at],
             dst_ref=other.at[at],
-            send_sem=x_send.at[i],
-            recv_sem=x_recv.at[part * pieces + h],
+            send_sem=sent_sem.at[kind],
+            recv_sem=arrival,
             device_id=device,
             device_id_type=MESH,
         )
 
+    def line_sem(part, h):
+        return x_recv.at[part // 2, h]
+
     def piece_arrived(part, h):
-        piece_copy(other, part, h, 0, sp=mate).wait_recv()
+        ref = other.at[piece_at(part, h)]
+        pltpu.make_async_copy(ref, ref, line_sem(part, h)).wait()
 
     across_part, along_part, diagonal_part = across * 2 + tp, along * 2 + tp, diagonal * 2 + tp
     relays = [(own_part, h, ("tp", "fs_across", "fs_along")) for h in range(pieces)]
@@ -465,9 +481,11 @@
     devices = {"tp": {"tp": twin}, "fs_across": {"fs": across}, "fs_along": {"fs": along}}
 
     def relay_copies(j):
-        base = sum(len(to) for _, _, to in relays[:j])
         part, h, to = relays[j]
-        return [piece_copy(other, part, h, base + i, **devices[d]) for i, d in enumerate(to)]
+        return [
+            piece_copy(other, part, h, RELAYED, twin_recv.at[0] if d == "tp" else line_sem(part, h), **devices[d])
+            for d in to
+        ]
 
     def relay(*which):
         for j in which:
@@ -486,92 +504,43 @@
 
     def pieces_out(*which):
         for h in which:
-            piece_copy(normed, own_part, h, h, sp=mate).start()
+            piece_copy(normed, own_part, h, RELAYED, line_sem(own_part, h), sp=mate).start()
 
     @pl.when(end)
     def _():
         pieces_out(*range(pieces))
-        send(True, me, K, V, Q, A, B, C)
+        send(True, me, K, V, Q, R, A, B, C)
 
     @pl.when(middle)
     def _():
-        send(False, me, K, V, Q, A, B, C)
-        send(True, me, K, V, Q)
-
+        send(False, me, K, V, Q, R, A, B, C, D)
+        send(True, me, K, V, Q, R)
+
+    others = tok.at[pl.ds(0, rows - part_rows)]
+    pltpu.make_async_copy(others, others, tok_sem.at[1]).wait()
     for i in range(1, parts):
         norm_part(i)
 
-    @pl.when(middle)
-    def _():
-        relay(OWN_X)
-        forward(True, peer, K, V)
-        relay(OWN_X + 1, ACROSS, ALONG)
-        forward(True, peer, Q)
-        relay(OWN_X + 2, ACROSS + 1, ALONG + 1, OWN_X + 3, ACROSS + 2, ALONG + 2)
-        forward(False, mate, K, V)
-        send(False, me, D, E)
-        relay(ACROSS + 3, ALONG + 3, DIAGONAL, DIAGONAL + 1)
-        forward(True, far, K, V)
-
-    @pl.when(end)
-    def _():
-        for shard in (mate, peer, far):
-            for u in (K, V):
-                arrived(u, shard)
-
     tile = 512
-
-    @pl.loop(0, rows // tile)
-    def _(i):
-        base = pl.multiple_of(i * tile, tile)
-        kv[pl.ds(base + WINDOW, tile), :] = lax.dot_general(
-            normed[pl.ds(base, tile), :], kv_all[...], (((1,), (1,)), ((), ())), preferred_element_type=f32
-        ).astype(bf16)
-
-    def halo(buffer, start, length, i):
-        return pltpu.make_async_remote_copy(
-            src_ref=buffer.at[pl.ds(start, length)],
-            dst_ref=buffer.at[pl.ds(0, length)],
-            send_sem=halo_send.at[i],
-            recv_sem=halo_recv.at[i],
-            device_id={"sp": right},
-            device_id_type=MESH,
-        )
-
-    kv_halo = halo(kv, rows, WINDOW, 0)
-
-    @pl.when(jnp.logical_not(has_left))
-    def _():
-        kv[pl.ds(0, WINDOW), :] = jnp.zeros((WINDOW, kv.shape[1]), bf16)
-
-    @pl.when(has_right)
-    def _():
-        kv_halo.start()
-
-    @pl.when(middle)
-    def _():
-        forward(False, mate, Q)
-
-    @pl.when(end)
-    def _():
-        send(True, me, D, E)
-        arrived(Q, mate)
-        arrived(Q, peer)
 
     early = pl.ds(pl.multiple_of(first * depth, depth), 3 * depth)
     late = pl.ds(pl.multiple_of(far * depth, depth), depth)
 
-    @pl.loop(0, rows // tile)
-    def _(i):
-        at = pl.ds(pl.multiple_of(i * tile, tile), tile)
-        q_part[at, :] = jnp.dot(normed[at, early], q_all[early, :], preferred_element_type=f32)
+    kv_halo = pltpu.make_async_remote_copy(
+        src_ref=kv.at[pl.ds(rows, WINDOW)],
+        dst_ref=kv.at[pl.ds(0, WINDOW)],
+        send_sem=sent_sem.at[HALO],
+        recv_sem=halo_recv.at[0],
+        device_id={"sp": right},
+        device_id_type=MESH,
+    )
 
     own_base, mate_base = jnp.where(me == 1, rows, 0), jnp.where(me == 1, 0, rows)
     bases = (own_base, mate_base)
     sources = (normed, other)
     tiles = rows // tile
     OWN, MATE = 0, 1
-    last = tiles - 1
+
     def tile_at(i):
         return pl.ds(i * tile if isinstance(i, int) else pl.multiple_of(i * tile, tile), tile)
 
@@ -580,7 +549,7 @@
         return pltpu.make_async_remote_copy(
             src_ref=conv_out.at[at],
             dst_ref=conv_back.at[at],
-            send_sem=out_send.at[g * tiles + i],
+            send_sem=sent_sem.at[RETURNED],
             recv_sem=out_recv.at[g * tiles + i],
             device_id={"sp": mate},
             device_id_type=MESH,
@@ -590,13 +559,14 @@
         return pltpu.make_async_remote_copy(
             src_ref=edge_out.at[g],
             dst_ref=edge_in.at[g],
-            send_sem=halo_send.at[1 + g],
+            send_sem=sent_sem.at[EDGES],
             recv_sem=halo_recv.at[1 + g],
             device_id={"sp": right},
             device_id_type=MESH,
         )
 
     center = pl.ds(depth, 2 * depth)
+    everything = pl.ds(0, conv_w.shape[1])
 
     def dot(which, tokens, start, length, at):
         return lax.dot_general(
@@ -606,14 +576,15 @@
             preferred_element_type=f32,
         )
 
-    def partial(which, u, v, at, fresh):
+    def partial(which, i, u, v, at, fresh=False):
         start = 2 * channel[u - A]
         span = pl.ds(start, 2 * channel[v - A] + 2 * widths[v - A] - start)
-        for i in range(tiles):
-            value = dot(which, tile_at(i), span.start, span.size, at)
-            sums[which, span, tile_at(i)] = value if fresh else sums[which, span, tile_at(i)] + value
+        value = dot(which, tile_at(i), span.start, span.size, at)
+        sums[which, span, tile_at(i)] = value if fresh else sums[which, span, tile_at(i)] + value
 
     def product(which, tokens, start, length):
+        if which == OWN and start == 2 * channel[-1]:
+            return dot(which, tokens, start, length, everything)
         return sums[which, pl.ds(start, length), tokens] + dot(which, tokens, start, length, late)
 
     def keep(g, at, value):
@@ -630,25 +601,21 @@
             total = total + turned_taps[of, k : k + 1] * moved[:, LANES:]
         return gate * total
 
-    def own_edge(g):
+    def mate_tiles(g):
         of = pl.ds(channel[g], widths[g])
         tokens = pl.ds(rows - LANES, LANES)
         keep(g, own_base + rows - LANES, product(OWN, tokens, 2 * channel[g], 2 * widths[g]))
-
-        @pl.when(me == 1)
-        def _():
-            conv_in[of, pl.ds(0, LANES)] = jnp.zeros((widths[g], LANES), f32)
-            edge = jnp.transpose(conv_in[of, pl.ds(2 * rows, LANES)])
-            edge_out[g, :, pl.ds(0, widths[g])] = edge[LANES - PAD :]
-            edge_copy(g).start()
-
-    def mate_tiles(g):
-        of = pl.ds(channel[g], widths[g])
         for i in range(tiles):
             at = mate_base + i * tile
             value = product(MATE, tile_at(i), 2 * channel[g], 2 * widths[g])
             conv_out[of, tile_at(i)] = convolve(g, at, keep(g, at, value)).astype(bf16)
             out_copy(g, i).start()
+
+        @pl.when(me == 1)
+        def _():
+            edge = jnp.transpose(conv_in[of, pl.ds(2 * rows, LANES)])
+            edge_out[g, :, pl.ds(0, widths[g])] = edge[LANES - PAD :]
+            edge_copy(g).start()
 
     def own_tiles(*which):
         @pl.when(me == 2)
@@ -679,24 +646,72 @@
 
     @pl.when(middle)
     def _():
-        relay(DIAGONAL + 2)
-        for u in units[A:]:
+        relay(OWN_X)
+        forward(True, peer, K, V)
+        relay(OWN_X + 1)
+        forward(True, peer, Q)
+        relay(ACROSS, ALONG)
+        forward(True, peer, R)
+        relay(OWN_X + 2, ACROSS + 1, ALONG + 1, OWN_X + 3)
+        forward(False, mate, K, V)
+        relay(ACROSS + 2, ALONG + 2)
+        forward(False, mate, Q)
+        relay(DIAGONAL, DIAGONAL + 1)
+        forward(False, mate, R)
+        for u in (A, B, C, D):
             arrived(u, peer)
-        partial(OWN, A, E, center, True)
+        partial(OWN, 0, A, D, center, True)
+        relay(ACROSS + 3, ALONG + 3)
+        forward(True, far, K, V)
         forward(False, mate, A)
-        relay(DIAGONAL + 3)
-        for part in (fs * 2 + twin, across * 2 + twin, along * 2 + twin, diagonal * 2 + twin):
-            for h in range(pieces):
-                piece_arrived(part, h)
-        partial(MATE, A, E, center, True)
+
+    @pl.when(end)
+    def _():
+        for shard in (mate, peer, far):
+            for u in (K, V):
+                arrived(u, shard)
+
+    @pl.loop(0, rows // tile)
+    def _(i):
+        base = pl.multiple_of(i * tile, tile)
+        kv[pl.ds(base + WINDOW, tile), :] = lax.dot_general(
+            normed[pl.ds(base, tile), :], kv_all[...], (((1,), (1,)), ((), ())), preferred_element_type=f32
+        ).astype(bf16)
+
+    @pl.when(jnp.logical_not(has_left))
+    def _():
+        kv[pl.ds(0, WINDOW), :] = jnp.zeros((WINDOW, kv.shape[1]), bf16)
+
+    @pl.when(has_right)
+    def _():
+        kv_halo.start()
+
+    @pl.when(middle)
+    def _():
+        forward(True, far, Q)
+        partial(OWN, 1, A, D, center, True)
         forward(False, mate, B)
-        for which in (OWN, MATE):
-            partial(which, A, B, shard_at(mate), False)
-        forward(True, far, Q)
 
     @pl.when(end)
     def _():
+        send(True, me, D, E)
+        for u in (Q, R):
+            arrived(u, mate)
+            arrived(u, peer)
+
+    @pl.loop(0, rows // tile)
+    def _(i):
+        at = pl.ds(pl.multiple_of(i * tile, tile), tile)
+        q_part[at, :] = jnp.dot(normed[at, early], q_all[early, :], preferred_element_type=f32)
+
+    @pl.when(middle)
+    def _():
+        forward(True, far, R)
+
+    @pl.when(end)
+    def _():
         arrived(Q, far)
+        arrived(R, far)
 
     @pl.loop(0, rows // tile)
     def _(i):
@@ -755,21 +770,42 @@
                 head = 2 * pair + side
                 log_ref[head : head + 1, pl.ds(base, WINDOW)] = turned_stats[row : row + 1]
 
-    services = (
-        lambda: forward(False, mate, C),
-        lambda: None,
-        lambda: forward(False, mate, D, E),
-    )
-    for i, job in enumerate(services):
-
-        @pl.loop(i * (blocks // 2 - 1) // 3, (i + 1) * (blocks // 2 - 1) // 3)
+    def finish(g):
+        arrived(A + g, far)
+        mate_tiles(g)
+
+    @pl.when(middle)
+    def _():
+        relay(DIAGONAL + 2, DIAGONAL + 3)
+        half_rows = other.at[pl.ds(0, rows // 2)]
+        pltpu.make_async_copy(half_rows, half_rows, twin_recv.at[0]).wait()
+        for i in range(tiles):
+            partial(MATE, i, A, D, center, True)
+        forward(False, mate, C)
+        send(False, me, E)
+        for which in (MATE, OWN):
+            for i in range(tiles):
+                partial(which, i, A, B, shard_at(mate))
+        finish(0)
+
+    def attend_pairs(start, stop):
+        @pl.loop(start, stop)
         def _(j):
             attend(2 * j + 1, band)
             attend(2 * j + 2, band)
 
-        @pl.when(middle)
-        def _():
-            job()
+    cut = (blocks // 2 - 1) * 2 // 3
+    attend_pairs(0, cut)
+
+    @pl.when(middle)
+    def _():
+        finish(1)
+
+    attend_pairs(cut, blocks // 2 - 1)
+
+    @pl.when(middle)
+    def _():
+        forward(False, mate, D, E)
 
     @pl.when(has_left)
     def _():
@@ -780,24 +816,21 @@
 
     @pl.when(middle)
     def _():
-        def finish(g):
-            arrived(A + g, far)
-            own_edge(g)
-            mate_tiles(g)
-
-        finish(0)
         for which in (MATE, OWN):
-            partial(which, C, E, shard_at(mate), False)
-        finish(1)
-        own_tiles(0, 1)
+            for i in range(tiles):
+                partial(which, i, C, D, shard_at(mate))
+        finish(2)
+        arrived(E, peer)
         for i in range(tiles):
-            mix(0, i, convolved)
-        finish(2)
+            partial(MATE, i, E, E, early, True)
         finish(3)
         finish(4)
-        own_tiles(2, 3, 4)
-        for i in range(tiles):
-            mix(1, i, convolved)
+        own_tiles(0, 1)
+        own_tiles(2, 3)
+        own_tiles(4)
+        for half in range(2):
+            for i in range(tiles):
+                mix(half, i, convolved)
 
     @pl.when(end)
     def _():
@@ -811,35 +844,24 @@
     def _():
         kv_halo.wait_send()
 
-    for u in (K, V, Q):
-        hop(u, me, True).wait_send()
+    attention_shard = depth * (2 * HEAD_DIM + width)
+    whole_shard = attention_shard + depth * 2 * width
 
     @pl.when(end)
     def _():
-        for h in range(pieces):
-            piece_copy(normed, own_part, h, h, sp=mate).wait_send()
-        for u in units[A:]:
-            hop(u, me, True).wait_send()
+        drain(TO_MATE, whole_shard)
+        drain(RELAYED, part_rows * other.shape[1])
 
     @pl.when(middle)
     def _():
-        for u in (K, V, Q):
-            hop(u, peer, True).wait_send()
-            hop(u, far, True).wait_send()
-        for u in units:
-            hop(u, me, False).wait_send()
-            hop(u, mate, False).wait_send()
-        for j in range(len(relays)):
-            for copy in relay_copies(j):
-                copy.wait_send()
-        for g in groups:
-            for i in range(tiles):
-                out_copy(g, i).wait_send()
+        drain(TO_MATE, 3 * attention_shard)
+        drain(TO_PEER, 2 * whole_shard)
+        drain(RELAYED, sum(len(to) for _, _, to in relays) * piece * other.shape[1])
+        pltpu.make_async_copy(conv_out, conv_out, sent_sem.at[RETURNED]).wait()
 
         @pl.when(me == 1)
         def _():
-            for g in groups:
-                edge_copy(g).wait_send()
+            pltpu.make_async_copy(edge_out, edge_out, sent_sem.at[EDGES]).wait()
 
 
 def paired_body(tokens, norm_gain, w_query, w_key, w_value, w_conv_in, w_conv_gate, conv_taps, sink_logits):
@@ -879,16 +901,13 @@
             pltpu.VMEM((width, 8), f32),
             pltpu.VMEM((5, PAD, LANES), f32),
             pltpu.VMEM((5, PAD, LANES), f32),
-            dma((8,)),
-            dma((5,)),
-            dma((8, 4)),
-            dma((8, 4)),
-            dma((8, 4)),
+            dma((2,)),
+            dma((3,)),
+            dma((9, 3)),
             dma((6,)),
             dma((6,)),
-            dma((28,)),
-            dma((32,)),
-            dma((5 * tiles,)),
+            dma((4, 4)),
+            dma((1,)),
             dma((5 * tiles,)),
         ],
         compiler_params=pltpu.CompilerParams(

time: 61 us -> 55 us (0.902)
  Pallas kernels: 58.8 us -> 52.8 us
    pallas_call x1, Pallas kernels: 58.8 us -> 52.8 us  [paired_body(): pl.pallas_call(paired_kernel, out_shape=(pltpu.VMEM((rows, width), bf16),...]
where the time goes in v5:
time: 55 us; the launch traced here: 54.8 us
  Pallas kernels  52.8 us (96%)
  local copies, waits for them, and re-layouts  1.4 us (3%)
  between operations  0.64 us (1%)
    pallas_call x1, Pallas kernels, paired_body(): pl.pallas_call(paired_kernel, out_shape=(pltpu.VMEM((rows, width), bf16),...  52.8 us
    unnamed x2, local copies, waits for them, and re-layouts  1.4 us

profile of v5, /device:TPU:0, one launch (start us, length us, event | category | flops | bytes accessed | tf_op | source)
XLA Modules:
  0.0 54.8 jit_solution(14849931183481649951)
XLA Ops:
  0.6 52.8 %paired_attend_convolve.1 = (bf16[1024,256]{1,0:T(8,128)(2,1)S(1)}, f32[4,1024]{1,0:T(4,128)S(1)}) custom-call(bf16[1024,2048]{1,0:T(8,128)(2,1)} %tok_ref.1, f32[1,2048]{1,0:T(1,128)} %bitcast.5, bf16[64,512]{1,0:T(8,128)(2,1)} %bitcast.3, bf16[64,512]{1,0:T(8,128)(2,1)} %bitcast.4, bf16[512,256]{1,0:T(8,128)(2,1)} %refs_2_.1, bf16[512,256]{1,0:T(8,128)(2,1)} %refs_3_.1, ...), custom_call_target="tpu_custom_call" | custom-call | tf_op jit(solution)/shard_map/paired_attend_convolve/pallas_call | solution.py:876
  53.4 0.8 %copy.13 = bf16[1024,256]{1,0:T(8,128)(2,1)} copy(bf16[1024,256]{1,0:T(8,128)(2,1)S(1)} %get-tuple-element.2) | data formatting | bytes 1048576
  54.2 0.6 %copy.14 = f32[4,1024]{1,0:T(4,128)} copy(f32[4,1024]{1,0:T(4,128)S(1)} %get-tuple-element.3) | data formatting | bytes 32768

commit v6 on v5

--- a/solution.py
+++ b/solution.py
@@ -315,6 +315,17 @@
             @pl.loop(me, n)
             def _(s):
                 hop(a, s, False).wait_send()
+
+
+def write_out(mixed_ref, log_ref, mixed_out, log_out, sems):
+    copies = [
+        pltpu.make_async_copy(mixed_ref, mixed_out, sems.at[0]),
+        pltpu.make_async_copy(log_ref, log_out, sems.at[1]),
+    ]
+    for copy in copies:
+        copy.start()
+    for copy in copies:
+        copy.wait()
 
 
 def paired_kernel(tok_ref, gain_ref, *refs):
@@ -364,8 +375,6 @@
     for i in range(parts):
         at = rows_of(part_at(i) * part_rows, part_rows)
         tok_copies.append(pltpu.make_async_copy(tok_ref.at[at], tok.at[at], tok_sem.at[min(i, 1)]))
-    for copy in tok_copies:
-        copy.start()
 
     def shard_at(shard):
         return pl.ds(pl.multiple_of(shard * depth, depth), depth)
@@ -381,7 +390,7 @@
     own_copies = [pltpu.make_async_copy(shards[u], place(u, me), own_sem.at[0]) for u in (K, V)]
     own_copies.append(pltpu.make_async_copy(shards[2], q_all.at[shard_at(me)], own_sem.at[1]))
     own_copies += [pltpu.make_async_copy(shards[3 + j], stage.at[j], own_sem.at[2]) for j in range(2)]
-    for copy in own_copies:
+    for copy in own_copies[:3] + tok_copies[:1] + own_copies[3:] + tok_copies[1:]:
         copy.start()
 
     def norm_part(i):
@@ -408,8 +417,103 @@
         greet(fs=along)
         greet(tp=twin)
 
+    pl.semaphore_wait(barrier, jnp.where(middle, 5, 1))
+
+    TO_MATE, TO_PEER, RELAYED, RETURNED, EDGES, HALO = range(6)
+
+    def slot(shard, device):
+        return shard - jnp.where(shard > device, 1, 0)
+
+    def source(u):
+        return shards[u] if u < Q else shards[2].at[:, pl.ds((u - Q) * LANES, LANES)]
+
+    def hop(u, shard, to_mate):
+        target = mate if to_mate else peer
+        return pltpu.make_async_remote_copy(
+            src_ref=source(u) if shard is me and u < A else place(u, shard),
+            dst_ref=place(u, shard),
+            send_sem=sent_sem.at[TO_MATE if to_mate else TO_PEER],
+            recv_sem=recv_sem.at[u, slot(shard, target)],
+            device_id={"sp": target},
+            device_id_type=MESH,
+        )
+
+    def arrived(u, shard):
+        ref = place(u, shard)
+        pltpu.make_async_copy(ref, ref, recv_sem.at[u, slot(shard, me)]).wait()
+
+    def drain(kind, elements):
+        ref = other.at[pl.ds(0, elements // other.shape[1])]
+        pltpu.make_async_copy(ref, ref, sent_sem.at[kind]).wait()
+
+    def piece_at(part, h):
+        return rows_of(part * part_rows + h * piece, piece)
+
+    def piece_copy(buffer, part, h, kind, arrival, **device):
+        at = piece_at(part, h)
+        return pltpu.make_async_remote_copy(
+            src_ref=buffer.at[at],
+            dst_ref=other.at[at],
+            send_sem=sent_sem.at[kind],
+            recv_sem=arrival,
+            device_id=device,
+            device_id_type=MESH,
+        )
+
+    def line_sem(part, h):
+        return x_recv.at[part // 2, h]
+
+    def piece_arrived(part, h):
+        ref = other.at[piece_at(part, h)]
+        pltpu.make_async_copy(ref, ref, line_sem(part, h)).wait()
+
+    across_part, along_part, diagonal_part = across * 2 + tp, along * 2 + tp, diagonal * 2 + tp
+    relays = [(own_part, h, ("tp", "fs_across", "fs_along")) for h in range(pieces)]
+    relays += [(across_part, h, ("tp", "fs_along")[: 2 - h % 2]) for h in range(pieces)]
+    relays += [(along_part, h, ("tp", "fs_across")[: 1 + h % 2]) for h in range(pieces)]
+    relays += [(diagonal_part, h, ("tp",)) for h in range(pieces)]
+    OWN_X, ACROSS, ALONG, DIAGONAL = (pieces * j for j in range(4))
+    devices = {"tp": {"tp": twin}, "fs_across": {"fs": across}, "fs_along": {"fs": along}}
+
+    def relay_copies(j):
+        part, h, to = relays[j]
+        return [
+            piece_copy(other, part, h, RELAYED, twin_recv.at[0] if d == "tp" else line_sem(part, h), **devices[d])
+            for d in to
+        ]
+
+    def relay(*which):
+        for j in which:
+            piece_arrived(relays[j][0], relays[j][1])
+            for copy in relay_copies(j):
+                copy.start()
+
+    def send(to_mate, shard, *which):
+        for u in which:
+            hop(u, shard, to_mate).start()
+
+    def forward(to_mate, shard, *which):
+        for u in which:
+            arrived(u, shard)
+            hop(u, shard, to_mate).start()
+
+    def pieces_out(*which):
+        for h in which:
+            piece_copy(normed, own_part, h, RELAYED, line_sem(own_part, h), sp=mate).start()
+
+    @pl.when(middle)
+    def _():
+        send(False, me, K, V, Q, R)
+        send(True, me, K, V, Q, R)
+
     tok_copies[0].wait()
     norm_part(0)
+
+    @pl.when(end)
+    def _():
+        pieces_out(*range(pieces))
+        send(True, me, K, V, Q, R)
+
     pltpu.make_async_copy(stage, stage, own_sem.at[2]).wait()
     for j in range(2):
         for block in range(depth // LANES):
@@ -420,101 +524,19 @@
                 conv_w[to, at] = turned[channel[g] : channel[g] + widths[g]]
     taps = taps_ref[...].astype(f32)
     turned_taps[...] = jnp.transpose(jnp.concatenate([taps, jnp.zeros((8 - TAPS, width), f32)], axis=0))
+    conv_in[:, pl.ds(0, LANES)] = jnp.zeros((width, LANES), f32)
+
+    @pl.when(end)
+    def _():
+        send(True, me, A, B, C)
+
+    @pl.when(middle)
+    def _():
+        send(False, me, A, B, C, D)
+
     own_kv = kv_all.at[:, shard_at(me)]
     pltpu.make_async_copy(own_kv, own_kv, own_sem.at[0]).wait()
     own_copies[2].wait()
-    conv_in[:, pl.ds(0, LANES)] = jnp.zeros((width, LANES), f32)
-
-    pl.semaphore_wait(barrier, jnp.where(middle, 5, 1))
-
-    TO_MATE, TO_PEER, RELAYED, RETURNED, EDGES, HALO = range(6)
-
-    def slot(shard, device):
-        return shard - jnp.where(shard > device, 1, 0)
-
-    def hop(u, shard, to_mate):
-        target = mate if to_mate else peer
-        return pltpu.make_async_remote_copy(
-            src_ref=place(u, shard),
-            dst_ref=place(u, shard),
-            send_sem=sent_sem.at[TO_MATE if to_mate else TO_PEER],
-            recv_sem=recv_sem.at[u, slot(shard, target)],
-            device_id={"sp": target},
-            device_id_type=MESH,
-        )
-
-    def arrived(u, shard):
-        ref = place(u, shard)
-        pltpu.make_async_copy(ref, ref, recv_sem.at[u, slot(shard, me)]).wait()
-
-    def drain(kind, elements):
-        ref = other.at[pl.ds(0, elements // other.shape[1])]
-        pltpu.make_async_copy(ref, ref, sent_sem.at[kind]).wait()
-
-    def piece_at(part, h):
-        return rows_of(part * part_rows + h * piece, piece)
-
-    def piece_copy(buffer, part, h, kind, arrival, **device):
-        at = piece_at(part, h)
-        return pltpu.make_async_remote_copy(
-            src_ref=buffer.at[at],
-            dst_ref=other.at[at],
-            send_sem=sent_sem.at[kind],
-            recv_sem=arrival,
-            device_id=device,
-            device_id_type=MESH,
-        )
-
-    def line_sem(part, h):
-        return x_recv.at[part // 2, h]
-
-    def piece_arrived(part, h):
-        ref = other.at[piece_at(part, h)]
-        pltpu.make_async_copy(ref, ref, line_sem(part, h)).wait()
-
-    across_part, along_part, diagonal_part = across * 2 + tp, along * 2 + tp, diagonal * 2 + tp
-    relays = [(own_part, h, ("tp", "fs_across", "fs_along")) for h in range(pieces)]
-    relays += [(across_part, h, ("tp", "fs_along")[: 2 - h % 2]) for h in range(pieces)]
-    relays += [(along_part, h, ("tp", "fs_across")[: 1 + h % 2]) for h in range(pieces)]
-    relays += [(diagonal_part, h, ("tp",)) for h in range(pieces)]
-    OWN_X, ACROSS, ALONG, DIAGONAL = (pieces * j for j in range(4))
-    devices = {"tp": {"tp": twin}, "fs_across": {"fs": across}, "fs_along": {"fs": along}}
-
-    def relay_copies(j):
-        part, h, to = relays[j]
-        return [
-            piece_copy(other, part, h, RELAYED, twin_recv.at[0] if d == "tp" else line_sem(part, h), **devices[d])
-            for d in to
-        ]
-
-    def relay(*which):
-        for j in which:
-            piece_arrived(relays[j][0], relays[j][1])
-            for copy in relay_copies(j):
-                copy.start()
-
-    def send(to_mate, shard, *which):
-        for u in which:
-            hop(u, shard, to_mate).start()
-
-    def forward(to_mate, shard, *which):
-        for u in which:
-            arrived(u, shard)
-            hop(u, shard, to_mate).start()
-
-    def pieces_out(*which):
-        for h in which:
-            piece_copy(normed, own_part, h, RELAYED, line_sem(own_part, h), sp=mate).start()
-
-    @pl.when(end)
-    def _():
-        pieces_out(*range(pieces))
-        send(True, me, K, V, Q, R, A, B, C)
-
-    @pl.when(middle)
-    def _():
-        send(False, me, K, V, Q, R, A, B, C, D)
-        send(True, me, K, V, Q, R)
 
     others = tok.at[pl.ds(0, rows - part_rows)]
     pltpu.make_async_copy(others, others, tok_sem.at[1]).wait()
@@ -567,6 +589,7 @@
 
     center = pl.ds(depth, 2 * depth)
     everything = pl.ds(0, conv_w.shape[1])
+    edge_tokens = pl.ds(rows - LANES, LANES)
 
     def dot(which, tokens, start, length, at):
         return lax.dot_general(
@@ -583,7 +606,7 @@
         sums[which, span, tile_at(i)] = value if fresh else sums[which, span, tile_at(i)] + value
 
     def product(which, tokens, start, length):
-        if which == OWN and start == 2 * channel[-1]:
+        if which == OWN and start == 2 * channel[-1] and tokens is not edge_tokens:
             return dot(which, tokens, start, length, everything)
         return sums[which, pl.ds(start, length), tokens] + dot(which, tokens, start, length, late)
 
@@ -603,8 +626,7 @@
 
     def mate_tiles(g):
         of = pl.ds(channel[g], widths[g])
-        tokens = pl.ds(rows - LANES, LANES)
-        keep(g, own_base + rows - LANES, product(OWN, tokens, 2 * channel[g], 2 * widths[g]))
+        keep(g, own_base + rows - LANES, product(OWN, edge_tokens, 2 * channel[g], 2 * widths[g]))
         for i in range(tiles):
             at = mate_base + i * tile
             value = product(MATE, tile_at(i), 2 * channel[g], 2 * widths[g])
@@ -783,10 +805,12 @@
             partial(MATE, i, A, D, center, True)
         forward(False, mate, C)
         send(False, me, E)
-        for which in (MATE, OWN):
-            for i in range(tiles):
-                partial(which, i, A, B, shard_at(mate))
+        for i in range(tiles):
+            partial(MATE, i, A, B, shard_at(mate))
+        partial(OWN, tiles - 1, A, B, shard_at(mate))
         finish(0)
+        for i in range(tiles - 1):
+            partial(OWN, i, A, B, shard_at(mate))
 
     def attend_pairs(start, stop):
         @pl.loop(start, stop)
@@ -799,32 +823,37 @@
 
     @pl.when(middle)
     def _():
+        forward(False, mate, D, E)
         finish(1)
 
     attend_pairs(cut, blocks // 2 - 1)
 
+    @pl.when(has_left)
+    def _():
+        kv_halo.wait_recv()
+
     @pl.when(middle)
     def _():
-        forward(False, mate, D, E)
-
-    @pl.when(has_left)
-    def _():
-        kv_halo.wait_recv()
-
-    attend(blocks - 1, band)
-    attend(0, band & ((key_idx >= WINDOW) | has_left))
-
-    @pl.when(middle)
-    def _():
-        for which in (MATE, OWN):
-            for i in range(tiles):
-                partial(which, i, C, D, shard_at(mate))
+        for i in range(tiles):
+            partial(MATE, i, C, D, shard_at(mate))
+        partial(OWN, tiles - 1, C, D, shard_at(mate))
         finish(2)
         arrived(E, peer)
         for i in range(tiles):
             partial(MATE, i, E, E, early, True)
+        sums[OWN, pl.ds(2 * channel[4], 2 * widths[4]), edge_tokens] = dot(
+            OWN, edge_tokens, 2 * channel[4], 2 * widths[4], early
+        )
         finish(3)
         finish(4)
+        for i in range(tiles - 1):
+            partial(OWN, i, C, D, shard_at(mate))
+
+    attend(blocks - 1, band)
+    attend(0, band & ((key_idx >= WINDOW) | has_left))
+
+    @pl.when(middle)
+    def _():
         own_tiles(0, 1)
         own_tiles(2, 3)
         own_tiles(4)
@@ -873,7 +902,7 @@
     smem = pl.BlockSpec(memory_space=pltpu.SMEM)
     dma = pltpu.SemaphoreType.DMA
     tiles = rows // 512
-    return pl.pallas_call(
+    results = pl.pallas_call(
         paired_kernel,
         out_shape=(
             pltpu.VMEM((rows, width), bf16),
@@ -915,6 +944,17 @@
         ),
         name="paired_attend_convolve",
     )(tokens, norm_gain.reshape(1, -1), w_key.T, w_value.T, w_query, w_conv_in, w_conv_gate, conv_taps, sink_logits)
+    return pl.pallas_call(
+        write_out,
+        out_shape=(
+            jax.ShapeDtypeStruct((rows, width), bf16),
+            jax.ShapeDtypeStruct((width // HEAD_DIM, rows), f32),
+        ),
+        in_specs=[vmem, vmem],
+        out_specs=(hbm, hbm),
+        scratch_shapes=[dma((2,))],
+        name="write_out",
+    )(*[pltpu.with_memory_space_constraint(result, pltpu.VMEM) for result in results])
 
 
 def line_body(n, tokens, norm_gain, w_query, w_key, w_value, w_conv_in, w_conv_gate, conv_taps, sink_logits):

time: 55 us -> 53.7 us (0.976)
  local copies, waits for them, and re-layouts: 1.4 us -> 0 us
    unnamed x2 -> x0, local copies, waits for them, and re-layouts: 1.4 us -> none
    pallas_call x0 -> x1, Pallas kernels: none -> 0.81 us  [paired_body(): pl.pallas_call(write_out, out_shape=(jax.ShapeDtypeStruct((rows, width),...]
    pallas_call x1, Pallas kernels: 52.8 us -> 52 us  [paired_body(): pl.pallas_call(paired_kernel, out_shape=(pltpu.VMEM((rows, width), bf16),...]
where the time goes in v6:
time: 53.7 us; the launch traced here: 53.5 us
  Pallas kernels  52.8 us (98%)
  between operations  0.64 us (1%)
    pallas_call x1, Pallas kernels, paired_body(): pl.pallas_call(paired_kernel, out_shape=(pltpu.VMEM((rows, width), bf16),...  52 us

profile of v6, /device:TPU:0, one launch (start us, length us, event | category | flops | bytes accessed | tf_op | source)
XLA Modules:
  0.0 53.5 jit_solution(9405214413604697796)
XLA Ops:
  0.6 52.0 %paired_attend_convolve.1 = (bf16[1024,256]{1,0:T(8,128)(2,1)S(1)}, f32[4,1024]{1,0:T(4,128)S(1)}) custom-call(bf16[1024,2048]{1,0:T(8,128)(2,1)} %tok_ref.1, f32[1,2048]{1,0:T(1,128)} %bitcast.5, bf16[64,512]{1,0:T(8,128)(2,1)} %bitcast.3, bf16[64,512]{1,0:T(8,128)(2,1)} %bitcast.4, bf16[512,256]{1,0:T(8,128)(2,1)} %refs_2_.1, bf16[512,256]{1,0:T(8,128)(2,1)} %refs_3_.1, ...), custom_call_target="tpu_custom_call" | custom-call | tf_op jit(solution)/shard_map/paired_attend_convolve/pallas_call | solution.py:905
  52.7 0.8 %write_out.1 = (bf16[1024,256]{1,0:T(8,128)(2,1)}, f32[4,1024]{1,0:T(4,128)}) custom-call(bf16[1024,256]{1,0:T(8,128)(2,1)S(1)} %get-tuple-element.4.mixed_ref, f32[4,1024]{1,0:T(4,128)S(1)} %get-tuple-element.5.log_ref), custom_call_target="tpu_custom_call" | custom-call | tf_op jit(solution)/shard_map/write_out/pallas_call | solution.py:947

commit v7 on v6

--- a/solution.py
+++ b/solution.py
@@ -328,10 +328,10 @@
         copy.wait()
 
 
-def paired_kernel(tok_ref, gain_ref, *refs):
+def paired_kernel(tok_ref, gain_in, *refs):
     shards = refs[:5]
     (
-        taps_ref, sink_ref, mixed_ref, log_ref,
+        taps_in, sink_in, mixed_ref, log_ref, gain_ref, taps_ref, sink_ref,
         tok, normed, other, kv_all, q_all, stage, conv_w, kv, query, q_part, attended,
         conv_in, convolved, sums, conv_out, conv_back, turned_taps, edge_out, edge_in,
         tok_sem, own_sem, recv_sem, sent_sem, halo_recv, x_recv, twin_recv, out_recv,
@@ -354,7 +354,7 @@
     depth = shards[2].shape[0]
     blocks = rows // WINDOW
     width = q_all.shape[1]
-    widths = (width // 4, width // 4, width // 4, width // 8, width // 8)
+    widths = (width // 4, width // 4, width * 5 // 16, width // 8, width // 16)
     groups = range(len(widths))
     channel = [sum(widths[:g]) for g in groups]
     K, V, Q, R, A, B, C, D, E = units = range(9)
@@ -390,7 +390,11 @@
     own_copies = [pltpu.make_async_copy(shards[u], place(u, me), own_sem.at[0]) for u in (K, V)]
     own_copies.append(pltpu.make_async_copy(shards[2], q_all.at[shard_at(me)], own_sem.at[1]))
     own_copies += [pltpu.make_async_copy(shards[3 + j], stage.at[j], own_sem.at[2]) for j in range(2)]
-    for copy in own_copies[:3] + tok_copies[:1] + own_copies[3:] + tok_copies[1:]:
+    small_copies = [
+        pltpu.make_async_copy(src, dst, own_sem.at[3 + j])
+        for j, (src, dst) in enumerate(((gain_in, gain_ref), (taps_in, taps_ref), (sink_in, sink_ref)))
+    ]
+    for copy in small_copies[:1] + tok_copies[:1] + own_copies + small_copies[1:] + tok_copies[1:]:
         copy.start()
 
     def norm_part(i):
@@ -417,7 +421,6 @@
         greet(fs=along)
         greet(tp=twin)
 
-    pl.semaphore_wait(barrier, jnp.where(middle, 5, 1))
 
     TO_MATE, TO_PEER, RELAYED, RETURNED, EDGES, HALO = range(6)
 
@@ -501,11 +504,14 @@
         for h in which:
             piece_copy(normed, own_part, h, RELAYED, line_sem(own_part, h), sp=mate).start()
 
+    pl.semaphore_wait(barrier, jnp.where(middle, 5, 1))
+
     @pl.when(middle)
     def _():
         send(False, me, K, V, Q, R)
         send(True, me, K, V, Q, R)
 
+    small_copies[0].wait()
     tok_copies[0].wait()
     norm_part(0)
 
@@ -522,6 +528,8 @@
             for g in groups:
                 to = pl.ds(2 * channel[g] + j * widths[g], widths[g])
                 conv_w[to, at] = turned[channel[g] : channel[g] + widths[g]]
+    small_copies[1].wait()
+    small_copies[2].wait()
     taps = taps_ref[...].astype(f32)
     turned_taps[...] = jnp.transpose(jnp.concatenate([taps, jnp.zeros((8 - TAPS, width), f32)], axis=0))
     conv_in[:, pl.ds(0, LANES)] = jnp.zeros((width, LANES), f32)
@@ -532,7 +540,7 @@
 
     @pl.when(middle)
     def _():
-        send(False, me, A, B, C, D)
+        send(False, me, A, B, C)
 
     own_kv = kv_all.at[:, shard_at(me)]
     pltpu.make_async_copy(own_kv, own_kv, own_sem.at[0]).wait()
@@ -572,7 +580,7 @@
             src_ref=conv_out.at[at],
             dst_ref=conv_back.at[at],
             send_sem=sent_sem.at[RETURNED],
-            recv_sem=out_recv.at[g * tiles + i],
+            recv_sem=out_recv.at[channel[g] // LANES * tiles + i],
             device_id={"sp": mate},
             device_id_type=MESH,
         )
@@ -582,7 +590,7 @@
             src_ref=edge_out.at[g],
             dst_ref=edge_in.at[g],
             send_sem=sent_sem.at[EDGES],
-            recv_sem=halo_recv.at[1 + g],
+            recv_sem=halo_recv.at[1],
             device_id={"sp": right},
             device_id_type=MESH,
         )
@@ -606,7 +614,7 @@
         sums[which, span, tile_at(i)] = value if fresh else sums[which, span, tile_at(i)] + value
 
     def product(which, tokens, start, length):
-        if which == OWN and start == 2 * channel[-1] and tokens is not edge_tokens:
+        if which == OWN and start >= 2 * channel[3] and tokens is not edge_tokens:
             return dot(which, tokens, start, length, everything)
         return sums[which, pl.ds(start, length), tokens] + dot(which, tokens, start, length, late)
 
@@ -644,7 +652,6 @@
         def _():
             for g in which:
                 of = pl.ds(channel[g], widths[g])
-                edge_copy(g).wait_recv()
                 edge = edge_in[g, :, pl.ds(0, widths[g])]
                 edge = jnp.concatenate([jnp.zeros((LANES - PAD, widths[g]), f32), edge], axis=0)
                 conv_in[of, pl.ds(0, LANES)] = jnp.transpose(edge)
@@ -680,9 +687,9 @@
         forward(False, mate, Q)
         relay(DIAGONAL, DIAGONAL + 1)
         forward(False, mate, R)
-        for u in (A, B, C, D):
+        for u in (A, B, C):
             arrived(u, peer)
-        partial(OWN, 0, A, D, center, True)
+        partial(OWN, 0, A, C, center, True)
         relay(ACROSS + 3, ALONG + 3)
         forward(True, far, K, V)
         forward(False, mate, A)
@@ -711,7 +718,7 @@
     @pl.when(middle)
     def _():
         forward(True, far, Q)
-        partial(OWN, 1, A, D, center, True)
+        partial(OWN, 1, A, C, center, True)
         forward(False, mate, B)
 
     @pl.when(end)
@@ -802,9 +809,9 @@
         half_rows = other.at[pl.ds(0, rows // 2)]
         pltpu.make_async_copy(half_rows, half_rows, twin_recv.at[0]).wait()
         for i in range(tiles):
-            partial(MATE, i, A, D, center, True)
+            partial(MATE, i, A, C, center, True)
         forward(False, mate, C)
-        send(False, me, E)
+        send(False, me, D, E)
         for i in range(tiles):
             partial(MATE, i, A, B, shard_at(mate))
         partial(OWN, tiles - 1, A, B, shard_at(mate))
@@ -835,28 +842,32 @@
     @pl.when(middle)
     def _():
         for i in range(tiles):
-            partial(MATE, i, C, D, shard_at(mate))
-        partial(OWN, tiles - 1, C, D, shard_at(mate))
+            partial(MATE, i, C, C, shard_at(mate))
+        partial(OWN, tiles - 1, C, C, shard_at(mate))
         finish(2)
+        arrived(D, peer)
         arrived(E, peer)
         for i in range(tiles):
-            partial(MATE, i, E, E, early, True)
-        sums[OWN, pl.ds(2 * channel[4], 2 * widths[4]), edge_tokens] = dot(
-            OWN, edge_tokens, 2 * channel[4], 2 * widths[4], early
-        )
+            partial(MATE, i, D, E, early, True)
+        late_rows = pl.ds(2 * channel[3], 2 * (widths[3] + widths[4]))
+        sums[OWN, late_rows, edge_tokens] = dot(OWN, edge_tokens, late_rows.start, late_rows.size, early)
         finish(3)
         finish(4)
         for i in range(tiles - 1):
-            partial(OWN, i, C, D, shard_at(mate))
+            partial(OWN, i, C, C, shard_at(mate))
 
     attend(blocks - 1, band)
     attend(0, band & ((key_idx >= WINDOW) | has_left))
 
     @pl.when(middle)
     def _():
+        @pl.when(me == 2)
+        def _():
+            pltpu.make_async_copy(edge_in, edge_in, halo_recv.at[1]).wait()
+
         own_tiles(0, 1)
-        own_tiles(2, 3)
-        own_tiles(4)
+        own_tiles(2)
+        own_tiles(3, 4)
         for half in range(2):
             for i in range(tiles):
                 mix(half, i, convolved)
@@ -865,8 +876,8 @@
     def _():
         for half in range(2):
             for i in range(tiles):
-                for g in (groups[:2], groups[2:])[half]:
-                    out_copy(g, i).wait_recv()
+                back = conv_back.at[pl.ds(half * LANES, LANES), tile_at(i)]
+                pltpu.make_async_copy(back, back, out_recv.at[half * tiles + i]).wait()
                 mix(half, i, conv_back)
 
     @pl.when(has_right)
@@ -899,7 +910,6 @@
     f32, bf16 = jnp.float32, jnp.bfloat16
     hbm = pl.BlockSpec(memory_space=pltpu.HBM)
     vmem = pl.BlockSpec(memory_space=pltpu.VMEM)
-    smem = pl.BlockSpec(memory_space=pltpu.SMEM)
     dma = pltpu.SemaphoreType.DMA
     tiles = rows // 512
     results = pl.pallas_call(
@@ -908,9 +918,12 @@
             pltpu.VMEM((rows, width), bf16),
             pltpu.VMEM((width // HEAD_DIM, rows), f32),
         ),
-        in_specs=[hbm, vmem] + [hbm] * 5 + [vmem, smem],
+        in_specs=[hbm] * 9,
         out_specs=(vmem, vmem),
         scratch_shapes=[
+            pltpu.VMEM((1, features), f32),
+            pltpu.VMEM(conv_taps.shape, bf16),
+            pltpu.SMEM((width // HEAD_DIM,), f32),
             pltpu.VMEM((rows, features), bf16),
             pltpu.VMEM((rows, features), bf16),
             pltpu.VMEM((rows, features), bf16),
@@ -931,13 +944,13 @@
             pltpu.VMEM((5, PAD, LANES), f32),
             pltpu.VMEM((5, PAD, LANES), f32),
             dma((2,)),
-            dma((3,)),
+            dma((6,)),
             dma((9, 3)),
             dma((6,)),
-            dma((6,)),
+            dma((2,)),
             dma((4, 4)),
             dma((1,)),
-            dma((5 * tiles,)),
+            dma((2 * tiles,)),
         ],
         compiler_params=pltpu.CompilerParams(
             collective_id=0, has_side_effects=True, vmem_limit_bytes=59 << 20

time: 53.7 us -> 52.6 us (0.980)
  Pallas kernels: 52.8 us -> 51.8 us
    pallas_call x1, Pallas kernels: 52 us -> 51 us  [paired_body(): pl.pallas_call(paired_kernel, out_shape=(pltpu.VMEM((rows, width), bf16),...]
where the time goes in v7:
time: 52.6 us; the launch traced here: 52.4 us
  Pallas kernels  51.8 us (98%)
  between operations  0.64 us (1%)
    pallas_call x1, Pallas kernels, paired_body(): pl.pallas_call(paired_kernel, out_shape=(pltpu.VMEM((rows, width), bf16),...  51 us

profile of v7, /device:TPU:0, one launch (start us, length us, event | category | flops | bytes accessed | tf_op | source)
XLA Modules:
  0.0 52.4 jit_solution(2199039677854493805)
XLA Ops:
  0.6 51.0 %paired_attend_convolve.1 = (bf16[1024,256]{1,0:T(8,128)(2,1)S(1)}, f32[4,1024]{1,0:T(4,128)S(1)}) custom-call(bf16[1024,2048]{1,0:T(8,128)(2,1)} %tok_ref.1, f32[1,2048]{1,0:T(1,128)} %bitcast.5, bf16[64,512]{1,0:T(8,128)(2,1)} %bitcast.3, bf16[64,512]{1,0:T(8,128)(2,1)} %bitcast.4, bf16[512,256]{1,0:T(8,128)(2,1)} %refs_2_.1, bf16[512,256]{1,0:T(8,128)(2,1)} %refs_3_.1, ...), custom_call_target="tpu_custom_call" | custom-call | tf_op jit(solution)/shard_map/paired_attend_convolve/pallas_call | solution.py:915
  51.6 0.8 %write_out.1 = (bf16[1024,256]{1,0:T(8,128)(2,1)}, f32[4,1024]{1,0:T(4,128)}) custom-call(bf16[1024,256]{1,0:T(8,128)(2,1)S(1)} %get-tuple-element.4.mixed_ref, f32[4,1024]{1,0:T(4,128)S(1)} %get-tuple-element.5.log_ref), custom_call_target="tpu_custom_call" | custom-call | tf_op jit(solution)/shard_map/write_out/pallas_call | solution.py:960

commit v8 on v7

--- a/solution.py
+++ b/solution.py
@@ -635,11 +635,14 @@
     def mate_tiles(g):
         of = pl.ds(channel[g], widths[g])
         keep(g, own_base + rows - LANES, product(OWN, edge_tokens, 2 * channel[g], 2 * widths[g]))
-        for i in range(tiles):
-            at = mate_base + i * tile
-            value = product(MATE, tile_at(i), 2 * channel[g], 2 * widths[g])
-            conv_out[of, tile_at(i)] = convolve(g, at, keep(g, at, value)).astype(bf16)
-            out_copy(g, i).start()
+        step = 1 if g < 3 else tiles
+        for start in range(0, tiles, step):
+            these = range(start, start + step)
+            values = [product(MATE, tile_at(i), 2 * channel[g], 2 * widths[g]) for i in these]
+            made = [keep(g, mate_base + i * tile, value) for i, value in zip(these, values)]
+            for i, gate in zip(these, made):
+                conv_out[of, tile_at(i)] = convolve(g, mate_base + i * tile, gate).astype(bf16)
+                out_copy(g, i).start()
 
         @pl.when(me == 1)
         def _():

time: 52.6 us -> 52.6 us (level)
  no operation moved by 1% of the time
where the time goes in v8:
time: 52.6 us; the launch traced here: 52.4 us
  Pallas kernels  51.8 us (98%)
  between operations  0.64 us (1%)
    pallas_call x1, Pallas kernels, paired_body(): pl.pallas_call(paired_kernel, out_shape=(pltpu.VMEM((rows, width), bf16),...  51 us

profile of v8, /device:TPU:0, one launch (start us, length us, event | category | flops | bytes accessed | tf_op | source)
XLA Modules:
  0.0 52.4 jit_solution(13301136378576681537)
XLA Ops:
  0.6 51.0 %paired_attend_convolve.1 = (bf16[1024,256]{1,0:T(8,128)(2,1)S(1)}, f32[4,1024]{1,0:T(4,128)S(1)}) custom-call(bf16[1024,2048]{1,0:T(8,128)(2,1)} %tok_ref.1, f32[1,2048]{1,0:T(1,128)} %bitcast.5, bf16[64,512]{1,0:T(8,128)(2,1)} %bitcast.3, bf16[64,512]{1,0:T(8,128)(2,1)} %bitcast.4, bf16[512,256]{1,0:T(8,128)(2,1)} %refs_2_.1, bf16[512,256]{1,0:T(8,128)(2,1)} %refs_3_.1, ...), custom_call_target="tpu_custom_call" | custom-call | tf_op jit(solution)/shard_map/paired_attend_convolve/pallas_call | solution.py:918
  51.6 0.8 %write_out.1 = (bf16[1024,256]{1,0:T(8,128)(2,1)}, f32[4,1024]{1,0:T(4,128)}) custom-call(bf16[1024,256]{1,0:T(8,128)(2,1)S(1)} %get-tuple-element.4.mixed_ref, f32[4,1024]{1,0:T(4,128)S(1)} %get-tuple-element.5.log_ref), custom_call_target="tpu_custom_call" | custom-call | tf_op jit(solution)/shard_map/write_out/pallas_call | solution.py:963
